TPU v7x, 512 devices: a whole 4x4x16 slice. The times are simulated.
512 devices in a mesh: ep: 32 (over z, core), tp: 16 (over y, x).
Axes of the slice: x: 4, y: 4, z: 16, core: 2. Of those that a mesh axis runs over, the one named last changes fastest.
Arguments:
- query_input: bfloat16 [16384, 2048], P('ep', 'tp'), may hold values from -6 to 6
- key_input: bfloat16 [16384, 1024], P('ep', 'tp'), may hold values from -6 to 6
- value_input: bfloat16 [16384, 1024], P('ep', 'tp'), may hold values from -64 to 64
- query_gain: float32 [64], replicated, may hold values from 0.5 to 6
- key_gain: float32 [64], replicated, may hold values from 0.5 to 6
- mixer_out: bfloat16 [2048, 4096], P(None, 'tp'), may hold values from -0.125 to 0.125
- moe_input: bfloat16 [8192, 4096], P('ep'), may hold values from -6 to 6
- moe_gain: float32 [4096], replicated, may hold values from 0.1 to 1.9
- routes: int32 [8192, 2], P('ep'), may hold values from 0 to 31, all different within a row; in each aligned block of 256 rows (0 to 255, 256 to 511, ...) at most 24 rows name the same one
- route_weight: float32 [8192, 2], P('ep'), may hold values from 0.1 to 1
- expert_gate: bfloat16 [32, 4096, 1024], P('ep', None, 'tp'), may hold values from -0.09375 to 0.09375
- expert_up: bfloat16 [32, 4096, 1024], P('ep', None, 'tp'), may hold values from -0.09375 to 0.09375
- expert_down: bfloat16 [32, 1024, 4096], P('ep', None, 'tp'), may hold values from -0.1875 to 0.1875
Outputs:
- attn_mixed: bfloat16 [16384, 4096], P('ep', 'tp')
- moe_out: bfloat16 [8192, 4096], P('ep', 'tp')
Inputs may be any that keep to these rules, and one draw needn't show every extreme that they name: `routes`: each row names 2 different experts. In the rows of one index of ep (aligned blocks of 256 rows) no expert is named by more than 24 rows, and in every draw some block has an expert named by exactly 24 rows.
All inputs are finite; a program needn't handle non-finite values.
Results may differ from a plain program's by a relative error of at most 0.0095.
The roundings to bfloat16 on the way count: a program that leaves them out, or rounds other values in their place, can miss the bound.
Values may be sent and summed in bfloat16 or wider, within the bound.
No kernel may reach another device: no remote copies, remote signals or barrier semaphores. Data moves between devices by JAX's collectives and lax.ppermute only.
A program may use at most 64 MiB of HBM per device.

v0:
```python
import math

import jax
import jax.numpy as jnp
from jax import lax
from jax.sharding import Mesh
from jax.sharding import PartitionSpec as P

GRID_W = 64
TP = ("tp_0", "tp_1")


epsilon = 1e-06
base_theta = 10000.0


def gather_axes(x, axes, dim):
    for axis in reversed(axes):
        x = lax.all_gather(x, axis, axis=dim, tiled=True)
    return x


def copy_for_each(x, axis):
    copies = jnp.broadcast_to(x, (lax.axis_size(axis), *x.shape))
    return lax.all_to_all(copies, axis, split_axis=0, concat_axis=0, tiled=True)


def joined_along(parts, dim):
    parts = jnp.moveaxis(parts, 0, dim)
    shape = parts.shape
    return parts.reshape(*shape[:dim], shape[dim] * shape[dim + 1], *shape[dim + 2 :])


def gathered_copies(x, axis, dim):
    parts = copy_for_each(x, axis)
    return joined_along(parts, dim)


def rope_tables(positions, head_width):
    quarter = head_width // 4
    inverse = base_theta ** (-jnp.arange(quarter, dtype=jnp.float32) / quarter)
    grid_row = (positions // GRID_W).astype(jnp.float32)
    grid_col = (positions % GRID_W).astype(jnp.float32)
    angles = jnp.concatenate(
        [grid_row[:, None] * inverse[None, :], grid_col[:, None] * inverse[None, :]], axis=1
    )
    return (jnp.cos(angles), jnp.sin(angles))


def head_norm(heads_in, gain):
    return (
        heads_in * lax.rsqrt(jnp.mean(heads_in * heads_in, axis=-1, keepdims=True) + epsilon) * gain
    )


def rotate(heads_in, cosine, sine_table):
    half_width = heads_in.shape[-1] // 2
    first_half = heads_in[..., :half_width]
    second_half = heads_in[..., half_width:]
    cos_rows = cosine[:, None, :]
    sin_rows = sine_table[:, None, :]
    return jnp.concatenate(
        [
            first_half * cos_rows - second_half * sin_rows,
            first_half * sin_rows + second_half * cos_rows,
        ],
        axis=-1,
    )


def slot_places(route_block, expert_count, capacity):
    flat_routes = route_block.reshape(-1)
    one_hot = (flat_routes[:, None] == jnp.arange(expert_count, dtype=jnp.int32)[None, :]).astype(
        jnp.int32
    )
    earlier = jnp.cumsum(one_hot, axis=0) - one_hot
    return flat_routes * capacity + jnp.sum(earlier * one_hot, axis=1)


def fill_sources(places, token_count, top_count, slot_total):
    source_rows = jnp.full((slot_total,), token_count, jnp.int32)
    pair_rows = jnp.arange(token_count * top_count, dtype=jnp.int32) // top_count
    return source_rows.at[places].set(pair_rows)


def on_device(
    query_input,
    key_input,
    value_input,
    query_gain,
    key_gain,
    mixer_out,
    moe_input,
    moe_gain,
    routes,
    route_weight,
    expert_gate,
    expert_up,
    expert_down,
):
    seq_dev = query_input.shape[0]
    head_width = query_gain.shape[0]
    heads_here = query_input.shape[1] // head_width
    key_heads_here = key_input.shape[1] // head_width
    group_size = heads_here // key_heads_here
    positions = lax.axis_index("ep") * seq_dev + jnp.arange(seq_dev, dtype=jnp.int32)
    cosine, sine_table = rope_tables(positions, head_width)
    query_heads = query_input.astype(jnp.float32).reshape(seq_dev, heads_here, head_width)
    key_heads = key_input.astype(jnp.float32).reshape(seq_dev, key_heads_here, head_width)
    query_rot = rotate(head_norm(query_heads, query_gain), cosine, sine_table).astype(jnp.bfloat16)
    query_rot = query_rot.reshape(seq_dev, key_heads_here, group_size, head_width)
    key_rot = rotate(head_norm(key_heads, key_gain), cosine, sine_table).astype(jnp.bfloat16)
    key_value = jnp.concatenate(
        [key_rot.reshape(seq_dev, key_heads_here * head_width), value_input], axis=1
    )
    score_scale = head_width ** (-0.5)
    initial = (
        jnp.full((key_heads_here, group_size, seq_dev), -jnp.inf, jnp.float32),
        jnp.zeros((key_heads_here, group_size, seq_dev), jnp.float32),
        jnp.zeros((seq_dev, key_heads_here, group_size, head_width), jnp.float32),
    )
    incoming = lax.all_gather(key_value, "ep", axis=0, tiled=True)
    incoming_rows = incoming.shape[0]
    block_len = math.gcd(incoming_rows, 512)
    key_blocks = incoming.reshape(
        incoming_rows // block_len, block_len, 2, key_heads_here, head_width
    )

    def one_block(current, key_block):
        largest, denominator, numerator = current
        scores = (
            jnp.einsum(
                "qkgd,skd->kgqs", query_rot, key_block[:, 0], preferred_element_type=jnp.float32
            )
            * score_scale
        )
        new_largest = jnp.maximum(largest, jnp.max(scores, axis=-1))
        weights = jnp.exp(scores - new_largest[..., None])
        factor = jnp.exp(largest - new_largest)
        denominator = denominator * factor + jnp.sum(weights, axis=-1)
        contribution = jnp.einsum(
            "kgqs,skd->qkgd",
            weights.astype(jnp.bfloat16),
            key_block[:, 1],
            preferred_element_type=jnp.float32,
        )
        numerator = numerator * jnp.transpose(factor, (2, 0, 1))[..., None] + contribution
        return ((new_largest, denominator, numerator), None)

    current, _ = lax.scan(one_block, initial, key_blocks)
    largest, denominator, numerator = current
    attended = numerator / jnp.transpose(denominator, (2, 0, 1))[..., None]
    attended = attended.reshape(seq_dev, heads_here * head_width).astype(jnp.bfloat16)
    projected = jnp.dot(gather_axes(attended, TP, 1), mixer_out, preferred_element_type=jnp.float32)
    attn_mixed = projected.astype(jnp.bfloat16)
    token_count, model_width = moe_input.shape
    top_count = routes.shape[1]
    local_experts = expert_gate.shape[0]
    senders = lax.axis_size("ep")
    expert_count = local_experts * senders
    capacity = 3 * token_count * top_count // (2 * expert_count)
    features = moe_input.astype(jnp.float32)
    normed = (
        features
        * lax.rsqrt(jnp.mean(features * features, axis=-1, keepdims=True) + epsilon)
        * moe_gain
    ).astype(jnp.bfloat16)
    places = slot_places(routes, expert_count, capacity)
    sources = fill_sources(places, token_count, top_count, expert_count * capacity)
    padded = jnp.concatenate([normed, jnp.zeros((1, model_width), jnp.bfloat16)], axis=0)
    column_width = expert_down.shape[2]
    feature_width = model_width // lax.axis_size(TP)
    own_columns = lax.dynamic_slice_in_dim(
        padded, lax.axis_index(TP) * feature_width, feature_width, 1
    )
    received = lax.all_to_all(own_columns[sources], "ep", split_axis=0, concat_axis=0, tiled=True)
    received = received.reshape(senders, local_experts, capacity, feature_width)
    incoming = lax.all_gather(received, TP, axis=3, tiled=True)
    gate_hidden = jnp.einsum(
        "sjcd,jdf->sjcf", incoming, expert_gate, preferred_element_type=jnp.float32
    )
    up_hidden = jnp.einsum(
        "sjcd,jdf->sjcf", incoming, expert_up, preferred_element_type=jnp.float32
    )
    hidden = (jax.nn.silu(gate_hidden) * up_hidden).astype(jnp.bfloat16)
    expert_out = jnp.einsum(
        "sjcf,jfd->sjcd",
        gathered_copies(hidden, TP, 3),
        expert_down,
        preferred_element_type=jnp.float32,
    )
    expert_out = expert_out.astype(jnp.bfloat16).reshape(
        senders * local_experts * capacity, column_width
    )
    returned = lax.all_to_all(expert_out, "ep", split_axis=0, concat_axis=0, tiled=True)
    picked = returned[places].reshape(token_count, top_count, column_width).astype(jnp.float32)
    shares = route_weight / jnp.sum(route_weight, axis=-1, keepdims=True)
    moe_out = jnp.sum(picked * shares[:, :, None], axis=1).astype(jnp.bfloat16)
    return (attn_mixed, moe_out)


def solution(mesh):
    torus = Mesh(mesh.devices.reshape(mesh.shape["ep"], 4, 4), ("ep", "tp_0", "tp_1"))
    placed = (
        P("ep", TP),
        P("ep", TP),
        P("ep", TP),
        P(),
        P(),
        P(None, TP),
        P("ep", None),
        P(),
        P("ep", None),
        P("ep", None),
        P("ep", None, TP),
        P("ep", None, TP),
        P("ep", None, TP),
    )
    return jax.shard_map(
        on_device,
        mesh=torus,
        in_specs=placed,
        out_specs=(P("ep", TP), P("ep", TP)),
        check_vma=False,
    )
```

profile of v0, /device:TPU:1, one launch (start us, length us, event | category | flops | bytes accessed | tf_op | source)
XLA Modules:
  0.0 329.3 jit_solution(3318978957161452941)
XLA Ops:
  9.6 1.5 pad_maximum_fusion
  14.8 2.4 scatter_custom_fusion
  18.6 3.3 gather_fusion
  21.9 16.7 %all-to-all-start = ((bf16[32,24,256]{2,1,0:T(8,128)(2,1)}), bf16[32,24,256]{2,1,0:T(8,128)(2,1)S(1)}, u32[]{:S(2)}, u32[]{:S(2)}) async-start(bf16[32,24,256]{2,1,0:T(8,128)(2,1)} %bitcast.14), calls=%async_computation | async-start | bytes 786432 | tf_op jit(solution)/shard_map/all_to_all | solution.py:176
  40.1 30.2 %all-to-all-done = bf16[32,24,256]{2,1,0:T(8,128)(2,1)S(1)} async-done(((bf16[32,24,256]{2,1,0:T(8,128)(2,1)}), bf16[32,24,256]{2,1,0:T(8,128)(2,1)S(1)}, u32[]{:S(2)}, u32[]{:S(2)}) %all-to-all-start) | async-done | bytes 393248 | tf_op jit(solution)/shard_map/all_to_all | solution.py:176
  71.2 30.8 %all-gather.5.cloned.1.call-done = bf16[16384,128]{0,1:T(8,128)(2,1)} async-done(((bf16[512,128]{0,1:T(8,128)(2,1)}), bf16[16384,128]{0,1:T(8,128)(2,1)}) %all-gather.5.cloned.1.call-update) | async-done | bytes 4194320 | tf_op jit(solution)/shard_map/all_gather | solution.py:122
  102.0 3.9 %copy.37 = bf16[16,8,32,512]{3,2,1,0:T(8,128)(2,1)S(1)} copy(bf16[16,8,32,512]{3,1,2,0:T(8,128)(2,1)} %bitcast.174) | data formatting | bytes 8388608
  105.9 4.4 %copy.28 = bf16[32,512,2,1,64]{1,4,2,3,0:T(8,128)(2,1)} copy(bf16[32,512,2,1,64]{1,0,4,2,3:T(8,128)(2,1)S(1)} %bitcast.172) | data formatting | bytes 8388608
  110.3 104.1 %while.15 = (s32[]{:T(128)}, f32[1,2,512]{2,1,0:T(2,128)S(1)}, f32[1,2,512]{2,1,0:T(2,128)S(1)}, f32[512,1,2,64]{0,3,2,1:T(8,128)S(1)}, bf16[32,512,2,1,64]{1,4,...) while((s32[]{:T(128)}, f32[1,2,512]{2,1,0:T(2,128)S(1)}, ...), condition=%wide.region_5.6_spmd.clone, body=%wide.region_2.5_spmd.clone.sunk | while | flops 138614784 | bytes 7405669 | solution.py:150
  114.5 1.4 bitcast_reduce_fusion.2
  117.8 1.4 bitcast_reduce_fusion.2
  121.0 1.4 bitcast_reduce_fusion.2
  124.3 1.4 bitcast_reduce_fusion.2
  127.5 1.4 bitcast_reduce_fusion.2
  130.8 1.4 bitcast_reduce_fusion.2
  137.3 1.4 bitcast_reduce_fusion.2
  140.5 1.4 bitcast_reduce_fusion.2
  143.8 1.4 bitcast_reduce_fusion.2
  147.0 1.4 bitcast_reduce_fusion.2
  150.3 1.4 bitcast_reduce_fusion.2
  156.8 1.4 bitcast_reduce_fusion.2
  160.1 1.4 bitcast_reduce_fusion.2
  163.3 1.4 bitcast_reduce_fusion.2
  166.6 1.4 bitcast_reduce_fusion.2
  169.8 1.4 bitcast_reduce_fusion.2
  173.1 1.4 bitcast_reduce_fusion.2
  176.4 1.4 bitcast_reduce_fusion.2
  179.6 1.4 bitcast_reduce_fusion.2
  182.9 1.4 bitcast_reduce_fusion.2
  186.1 1.4 bitcast_reduce_fusion.2
  195.9 1.4 bitcast_reduce_fusion.2
  208.9 1.4 bitcast_reduce_fusion.2
  214.5 4.8 %convolution_bitcast_fusion.2 = f32[32,1,24,64]{3,2,0,1:T(8,128)S(1)} fusion(bf16[32,24,4096]{2,1,0:T(8,128)(2,1)} %all-gather.9.cloned.1.call-done, bf16[1,4096,64]{1,2,0:T(8,128)(2,1)} %param.25), kind=kOutput, calls=%fused_computation.35 | convolution fusion | flops 402653184 | bytes 7012352 | tf_op jit(solution)/shard_map/sjcd,jdf->sjcf/dot_general | solution.py:179
  219.4 1.9 fusion.17
  221.3 2.3 broadcast_bitcast_fusion
  223.6 4.9 %reshape.442 = bf16[16,2,24576]{2,1,0:T(2,128)(2,1)} reshape(bf16[16,1,32,24,64]{4,3,2,1,0:T(8,128)(2,1)} %broadcast_bitcast_fusion) | data formatting | bytes 3145728
  228.5 6.3 %all-to-all-start.1 = ((bf16[16,2,24576]{2,1,0:T(2,128)(2,1)}), bf16[16,2,24576]{2,1,0:T(2,128)(2,1)S(1)}, u32[]{:S(2)}, u32[]{:S(2)}) async-start(bf16[16,2,24576]{2,1,0:T(2,128)(2,1)} %reshape.442), calls=%async_computation.1 | async-start | bytes 3145728 | tf_op jit(solution)/shard_map/all_to_all | solution.py:25
  235.0 29.6 %all_gather.13 = bf16[512,512]{0,1:T(8,128)(2,1)} all-gather(bf16[512,128]{0,1:T(8,128)(2,1)S(1)} %bitcast.177), channel_id=1, replica_groups=mesh['ep'=32,'tp_0'=4,'tp_1'=4] {'tp_1'}, dimensions={1}, use_global_device_ids=true | all-gather | bytes 655360 | tf_op jit(solution)/shard_map/all_gather | solution.py:19
  264.6 3.3 %reshape.443 = bf16[16,1,32,24,64]{4,3,2,1,0:T(8,128)(2,1)} reshape(bf16[16,2,24576]{2,1,0:T(2,128)(2,1)S(1)} %all-to-all-done.1) | data formatting | bytes 3145728
  268.0 2.6 bitcast_bitcast_fusion.1
  270.5 5.3 %copy.33 = bf16[32,1,24,16,64]{4,3,2,0,1:T(8,128)(2,1)} copy(bf16[32,1,24,16,64]{4,2,0,1,3:T(8,128)(2,1)S(1)} %bitcast_bitcast_fusion.1) | data formatting | bytes 3145728 | tf_op jit(solution)/shard_map/transpose | solution.py:29
  275.8 4.6 %reshape.398 = bf16[32,24,1024]{2,1,0:T(8,128)(2,1)S(1)} reshape(bf16[32,1,24,16,64]{4,3,2,0,1:T(8,128)(2,1)} %copy.33) | data formatting | bytes 3145728 | tf_op jit(solution)/shard_map/reshape.35
  281.8 9.7 %all-to-all-start.2 = ((bf16[32,24,256]{2,1,0:T(8,128)(2,1)}), bf16[32,24,256]{2,1,0:T(8,128)(2,1)S(1)}, u32[]{:S(2)}, u32[]{:S(2)}) async-start(bf16[32,24,256]{2,1,0:T(8,128)(2,1)} %convolution_convert_fusion), calls=%async_computation.2 | async-start | bytes 786432 | tf_op jit(solution)/shard_map/all_to_all | solution.py:195
  291.6 8.6 %all-gather.7.cloned.1.call-done = bf16[512,2048]{0,1:T(8,128)(2,1)} async-done(((bf16[512,512]{0,1:T(8,128)(2,1)}), bf16[512,2048]{0,1:T(8,128)(2,1)}) %all-gather.7.cloned.1.call-update) | async-done | bytes 2097168 | tf_op jit(solution)/shard_map/all_gather | solution.py:19
  300.2 3.0 convolution_convert_fusion.1
  303.3 15.9 %all-to-all-done.2 = bf16[32,24,256]{2,1,0:T(8,128)(2,1)S(1)} async-done(((bf16[32,24,256]{2,1,0:T(8,128)(2,1)}), bf16[32,24,256]{2,1,0:T(8,128)(2,1)S(1)}, u32[]{:S(2)}, u32[]{:S(2)}) %all-to-all-start.2) | async-done | bytes 393248 | tf_op jit(solution)/shard_map/all_to_all | solution.py:195
  319.2 1.9 gather_fusion.1
  321.4 1.4 multiply_reduce_fusion
  (273 shorter events, 82.3 us)
Async XLA Ops:
  7.2 293.1 %copy-start = (bf16[2048,256]{1,0:T(8,128)(2,1)S(1)}, bf16[2048,256]{1,0:T(8,128)(2,1)}, u32[]{:S(2)}) copy-start(bf16[2048,256]{1,0:T(8,128)(2,1)} %param.20) | copy-start | bytes 3145732
  7.2 10.1 %copy-start.1 = (bf16[256,4096]{1,0:T(8,128)(2,1)S(1)}, bf16[256,4096]{1,0:T(8,128)(2,1)}, u32[]{:S(2)}) copy-start(bf16[256,4096]{1,0:T(8,128)(2,1)} %param.21) | copy-start | bytes 6291460
  7.2 94.8 %all-gather.5.cloned.1.call-start = ((), (), s32[]{:S(2)}) async-start(), calls=%async_computation.3 | async-start | bytes 4325376 | tf_op jit(solution)/shard_map/all_gather | solution.py:122
  8.3 9.5 %copy-start.4 = (f32[4096]{0:T(1024)S(1)}, f32[4096]{0:T(1024)}, u32[]{:S(2)}) copy-start(f32[4096]{0:T(1024)} %param.22) | copy-start | bytes 49156
  18.6 20.3 %copy-start.3 = (bf16[512,128]{1,0:T(8,128)(2,1)S(1)}, bf16[512,128]{1,0:T(8,128)(2,1)}, u32[]{:S(2)}) copy-start(bf16[512,128]{1,0:T(8,128)(2,1)} %param.15) | copy-start | bytes 393220
  18.6 20.7 %copy-start.6 = (f32[64]{0:T(128)S(1)}, f32[64]{0:T(128)}, u32[]{:S(2)}) copy-start(f32[64]{0:T(128)} %param.18) | copy-start | bytes 772
  21.9 48.5 %all-to-all-start = ((bf16[32,24,256]{2,1,0:T(8,128)(2,1)}), bf16[32,24,256]{2,1,0:T(8,128)(2,1)S(1)}, u32[]{:S(2)}, u32[]{:S(2)}) async-start(bf16[32,24,256]{2,1,0:T(8,128)(2,1)} %bitcast.14), calls=%async_computation | async-start | bytes 786432 | tf_op jit(solution)/shard_map/all_to_all | solution.py:176
  38.6 175.9 %all-gather.9.cloned.1.call-start = ((), (), s32[]{:S(2)}) async-start(), calls=%async_computation.5 | async-start | bytes 6684672 | tf_op jit(solution)/shard_map/all_gather | solution.py:178
  70.4 0.8 copy-start.2
  214.4 4.8 %copy-start.8 = (bf16[1,4096,64]{1,2,0:T(8,128)(2,1)S(1)}, bf16[1,4096,64]{1,2,0:T(8,128)(2,1)}, u32[]{:S(2)}) copy-start(bf16[1,4096,64]{1,2,0:T(8,128)(2,1)} %param.26) | copy-start | bytes 1572868
  214.5 4.9 %copy-start.7 = (bf16[32,24,4096]{2,1,0:T(8,128)(2,1)S(1)}, bf16[32,24,4096]{2,1,0:T(8,128)(2,1)}, u32[]{:S(2)}) copy-start(bf16[32,24,4096]{2,1,0:T(8,128)(2,1)} %all-gather.9.cloned.1.call-done) | copy-start | bytes 18874372
  228.5 36.1 %all-to-all-start.1 = ((bf16[16,2,24576]{2,1,0:T(2,128)(2,1)}), bf16[16,2,24576]{2,1,0:T(2,128)(2,1)S(1)}, u32[]{:S(2)}, u32[]{:S(2)}) async-start(bf16[16,2,24576]{2,1,0:T(2,128)(2,1)} %reshape.442), calls=%async_computation.1 | async-start | bytes 3145728 | tf_op jit(solution)/shard_map/all_to_all | solution.py:25
  234.9 65.3 %all-gather.7.cloned.1.call-start = ((), (), s32[]{:S(2)}) async-start(), calls=%async_computation.4 | async-start | bytes 2621440 | tf_op jit(solution)/shard_map/all_gather | solution.py:19
  275.8 4.6 %copy-start.9 = (bf16[1,1024,256]{2,1,0:T(8,128)(2,1)S(1)}, bf16[1,1024,256]{2,1,0:T(8,128)(2,1)}, u32[]{:S(2)}) copy-start(bf16[1,1024,256]{2,1,0:T(8,128)(2,1)} %param.27) | copy-start | bytes 1572868
  280.4 11.0 %copy-start.5 = (f32[256,2]{0,1:T(2,128)S(1)}, f32[256,2]{0,1:T(2,128)}, u32[]{:S(2)}) copy-start(f32[256,2]{0,1:T(2,128)} %param.24) | copy-start | bytes 6148
  281.8 37.4 %all-to-all-start.2 = ((bf16[32,24,256]{2,1,0:T(8,128)(2,1)}), bf16[32,24,256]{2,1,0:T(8,128)(2,1)S(1)}, u32[]{:S(2)}, u32[]{:S(2)}) async-start(bf16[32,24,256]{2,1,0:T(8,128)(2,1)} %convolution_convert_fusion), calls=%async_computation.2 | async-start | bytes 786432 | tf_op jit(solution)/shard_map/all_to_all | solution.py:195
Sparse Core Ops, SparseCore 0:
  11.2 90.6 all-gather.4
  105.0 76.9 all-gather.8
  264.7 35.4 all-gather.6
where the time goes:
time: 331 us; the launch traced here: 329 us
  waiting for transfers between devices  85.6 us (26%)
  local copies, waits for them, and re-layouts  71.6 us (22%)
  matrix products  71.3 us (22%)
  starting transfers between devices  33 us (10%)
  blocking collectives  29.6 us (9%)
  other arithmetic  22.3 us (7%)
  between operations  14.2 us (4%)
    dot_general x32, matrix products, one_block(): jnp.einsum('qkgd,skd->kgqs', query_rot, key_block[:, 0], preferred_elemen...  43.9 us
    all_gather x1, waiting for transfers between devices, on_device(): incoming = lax.all_gather(key_value, 'ep', axis=0, tiled=True)  30.8 us
    all_to_all x1, waiting for transfers between devices, on_device(): lax.all_to_all(own_columns[sources], 'ep', split_axis=0, concat_axis=0, t...  30.2 us
    all_gather x1, blocking collectives, gather_axes(): x = lax.all_gather(x, axis, axis=dim, tiled=True)  29.6 us
    squeeze x32, local copies, waits for them, and re-layouts, on_device(): current, _ = lax.scan(one_block, initial, key_blocks)  29.4 us
    unnamed x26, local copies, waits for them, and re-layouts  20.6 us
    all_to_all x1, starting transfers between devices, on_device(): lax.all_to_all(own_columns[sources], 'ep', split_axis=0, concat_axis=0, t...  16.7 us
    dot_general x32, matrix products, one_block(): jnp.einsum('kgqs,skd->qkgd', weights.astype(jnp.bfloat16), key_block[:, 1...  16.3 us
  transfers between devices with their start and end apart: 6, of which 4 were waited for; matrix products, arithmetic and copies ran while one was open for 43% of the time, Pallas kernels for 0%

commit v1 on v0

v1 whole, which is shorter than its diff:
```python
import jax
import jax.numpy as jnp
from jax import lax
from jax.experimental import pallas as pl
from jax.experimental.pallas import tpu as pltpu
from jax.sharding import Mesh
from jax.sharding import PartitionSpec as P

GRID_W = 64
EP = ("z", "core")
TP = ("y", "x")
EPS = 1e-06
BASE = 10000.0
LOG2E = 1.4426950408889634

bf16 = jnp.bfloat16
f32 = jnp.float32


def dot(a, b):
    return jnp.dot(a, b, preferred_element_type=f32)


def params(mib=16):
    return pltpu.CompilerParams(vmem_limit_bytes=mib << 20)


def start_copies(pairs, sems):
    copies = [pltpu.make_async_copy(a, b, sems.at[i]) for i, (a, b) in enumerate(pairs)]
    for copy in copies:
        copy.start()
    return copies


def norm_turn(x, gain, cos, sin):
    half = x.shape[0] // 2
    x = x * lax.rsqrt(jnp.mean(x * x, axis=0, keepdims=True) + EPS) * gain
    a, b = x[:half], x[half:]
    return jnp.concatenate([a * cos - b * sin, a * sin + b * cos], axis=0)


def column(row):
    n = row.shape[1]
    same = lax.broadcasted_iota(jnp.int32, (n, n), 0) == lax.broadcasted_iota(
        jnp.int32, (n, n), 1
    )
    return jnp.sum(jnp.where(same, row, 0.0), axis=1, keepdims=True)


def key_body(
    k_hbm, v_hbm, gain_hbm, cos_ref, sin_ref, chunk_ref, k_ref, v_ref, gain_ref, sems
):
    for copy in start_copies(((k_hbm, k_ref), (v_hbm, v_ref), (gain_hbm, gain_ref)), sems):
        copy.wait()
    hw, n = k_ref.shape
    k_t = norm_turn(k_ref[...].astype(f32), column(gain_ref[...]), cos_ref[...], sin_ref[...])
    k_t = k_t.astype(bf16).astype(f32)
    packed = jnp.concatenate([k_t[:, : n // 2], k_t[:, n // 2 :]], axis=0)
    chunk_ref[: n // 2, :] = packed.T.astype(bf16)
    for j in range(n // 128):
        chunk_ref[n // 2 + hw * j : n // 2 + hw * (j + 1), :] = v_ref[:, 128 * j : 128 * (j + 1)]


def query_body(q_ref, gain_ref, cos_ref, sin_ref, qt_ref):
    n = q_ref.shape[0]
    hw = gain_ref.shape[1]
    q_t = q_ref[...].astype(f32).T
    gain = column(gain_ref[...])
    for h in range(q_t.shape[0] // hw):
        turned = norm_turn(q_t[hw * h : hw * (h + 1)], gain, cos_ref[...], sin_ref[...])
        scaled = turned.astype(bf16).astype(f32) * (hw**-0.5)
        qt_ref[:, n * h : n * (h + 1)] = scaled.astype(bf16)


def attend_body(
    qt_ref, kv_ref, out_ref, qlo_ref, qhi_ref, m_ref, acc_ref, s_ref, p_ref, *, n, hw, tile
):
    step = pl.program_id(0)
    cols = qt_ref.shape[1]
    half = n // 2

    @pl.when(step == 0)
    def _():
        zero = jnp.zeros((hw, cols), bf16)
        qlo_ref[:hw, :] = qt_ref[...]
        qlo_ref[hw:, :] = zero
        qhi_ref[:hw, :] = zero
        qhi_ref[hw:, :] = qt_ref[...]
        m_ref[...] = jnp.full(m_ref.shape, -1e30, f32)
        acc_ref[...] = jnp.zeros(acc_ref.shape, f32)

    ones = jnp.ones((16, half), bf16)
    units = [(c, t) for c in range(kv_ref.shape[0] // n) for t in range(cols // tile)]
    shrink = {}

    def scores(u):
        c, t = units[u]
        at = pl.ds(tile * t, tile)
        k_pack = kv_ref[n * c : n * c + half, :]
        s_ref[u % 2, :half, :] = dot(k_pack, qlo_ref[:, at])
        s_ref[u % 2, half:, :] = dot(k_pack, qhi_ref[:, at])

    def weights(u):
        at = pl.ds(tile * units[u][1], tile)
        s = s_ref[u % 2]
        old = m_ref[:, at]
        new = jnp.maximum(old, jnp.max(s, axis=0, keepdims=True) * LOG2E)
        m_ref[:, at] = new
        shrink[u] = jnp.exp2(old - new)
        p_ref[u % 2] = jnp.exp2(s * LOG2E - new).astype(bf16)

    def values(u):
        c, t = units[u]
        at = pl.ds(tile * t, tile)
        base = n * c + half
        v = [kv_ref[base + hw * j : base + hw * (j + 1), :] for j in range(4)]
        v_a = jnp.concatenate([jnp.concatenate(v[:2], axis=1), ones], axis=0)
        v_b = jnp.concatenate([jnp.concatenate(v[2:], axis=1), ones], axis=0)
        term = dot(v_a, p_ref[u % 2, :half, :]) + dot(v_b, p_ref[u % 2, half:, :])
        acc_ref[:, at] = acc_ref[:, at] * shrink[u] + term

    for i in range(len(units) + 2):
        if i < len(units):
            scores(i)
        if i >= 2:
            values(i - 2)
        if 1 <= i <= len(units):
            weights(i - 1)

    @pl.when(step == pl.num_programs(0) - 1)
    def _():
        acc = acc_ref[...]
        out = acc[:hw] / acc[hw : hw + 1]
        heads = cols // n
        stacked = jnp.concatenate([out[:, n * h : n * (h + 1)] for h in range(heads)], axis=0)
        out_ref[...] = stacked.T.astype(bf16)


def weights_body(at_ref, w0, w1, w2, w3, after_ref, out_ref):
    del after_ref
    x = at_ref[1]
    count = out_ref.shape[0]
    width = out_ref.shape[1] // count
    for j, w_ref in enumerate((w0, w1, w2, w3)):
        for d in range(count):
            row = pl.multiple_of((x ^ d) * width, width)
            out_ref[j, width * d : width * (d + 1), :] = w_ref[pl.ds(row, width), :]


def mixer_body(a0, a1, a2, a3, w_ref, own_ref, p1_ref, p2_ref, p3_ref):
    near = jnp.concatenate([a0[...], a1[...]], axis=1)
    far = jnp.concatenate([a2[...], a3[...]], axis=1)
    half = near.shape[1]
    for j, out_ref in enumerate((own_ref, p1_ref, p2_ref, p3_ref)):
        acc = dot(near, w_ref[j, :half, :]) + dot(far, w_ref[j, half:, :])
        out_ref[...] = acc.astype(out_ref.dtype)


def mixed_body(own_ref, r1_ref, r2_ref, r3_ref, out_ref):
    total = own_ref[...]
    for ref in (r1_ref, r2_ref, r3_ref):
        total = total + ref[...].astype(f32)
    out_ref[...] = total.astype(bf16)


def dispatch_body(
    at_ref, x_hbm, gain_hbm, routes_hbm, out_ref, x_ref, gain_ref, routes_ref, sems, *, experts, cap
):
    pairs = ((routes_hbm, routes_ref), (x_hbm, x_ref), (gain_hbm, gain_ref))
    copies = start_copies(pairs, sems)
    rows = x_ref.shape[0]
    copies[0].wait()
    ids = lax.broadcasted_iota(jnp.int32, (experts, rows), 0)
    hits = jnp.zeros((experts, rows), f32)
    for k in range(routes_ref.shape[0]):
        hits = hits + (ids == routes_ref[k : k + 1, :]).astype(f32)
    before = lax.broadcasted_iota(jnp.int32, (rows, rows), 0) < lax.broadcasted_iota(
        jnp.int32, (rows, rows), 1
    )
    rank = dot(hits.astype(bf16), before.astype(f32).astype(bf16))
    marks = (hits * (rank + 1.0)).astype(bf16)
    slots = experts * cap
    slot_row = lax.broadcasted_iota(jnp.int32, (slots, experts), 0)
    slot_exp = lax.broadcasted_iota(jnp.int32, (slots, experts), 1)
    spread = ((slot_row >= slot_exp * cap) & (slot_row < (slot_exp + 1) * cap)).astype(f32)
    wide = dot(spread.astype(bf16), marks)
    place = lax.broadcasted_iota(jnp.int32, (slots, rows), 0)
    want = (lax.rem(place, jnp.full_like(place, cap)) + 1).astype(f32)
    pick = (wide == want).astype(f32).astype(bf16)
    copies[1].wait()
    copies[2].wait()
    x = x_ref[...].astype(f32)
    width = out_ref.shape[1]
    own = pl.ds(pl.multiple_of(at_ref[0] * width, width), width)
    scale = lax.rsqrt(jnp.mean(x * x, axis=-1, keepdims=True) + EPS)
    normed = (x_ref[:, own].astype(f32) * scale * gain_ref[:, own]).astype(bf16)
    out_ref[...] = dot(pick, normed).astype(bf16)


def spread_body(x_ref, *refs):
    out_ref = refs[-1]
    cores, copies = 2, out_ref.shape[0] // 2
    count, rows, width = x_ref.shape
    cap = rows // cores
    x = x_ref[...].astype(f32)
    for c in range(cores):
        part = x[:, cap * c : cap * (c + 1), :].reshape(count * cap, width).astype(bf16)
        for i in range(copies):
            out_ref[copies * c + i] = part


def gate_up_body(at_ref, x_ref, w0_ref, w1_ref, w2_ref, w3_ref, *refs):
    out_ref = refs[-1]
    _, rows, width = x_ref.shape
    y = at_ref[0]
    ws = (w0_ref, w1_ref, w2_ref, w3_ref)
    blocks = w0_ref.shape[1] // width
    for j in range(0, len(ws), 2):
        for c in range(x_ref.shape[0] // blocks):
            acc = None
            for b in range(blocks):
                cols = slice(width * b, width * (b + 1))
                w = jnp.concatenate([ws[j][:, cols], ws[j + 1][:, cols]], axis=0)
                term = lax.dot_general(
                    x_ref[blocks * c + b], w, (((1,), (1,)), ((), ())), preferred_element_type=f32
                )
                acc = term if acc is None else acc + term
            half = acc.shape[1] // 2
            at = slice(rows * c, rows * (c + 1))
            out_ref[y ^ j, at, :] = acc[:, :half].astype(bf16)
            out_ref[y ^ (j + 1), at, :] = acc[:, half:].astype(bf16)


def hidden_body(parts_ref, out_ref):
    total = parts_ref[0].astype(f32)
    for j in range(1, parts_ref.shape[0]):
        total = total + parts_ref[j].astype(f32)
    hid = total.shape[1] // 2
    gate = total
    up = pltpu.roll(total, hid, 1)
    value = gate / (1.0 + jnp.exp(-gate)) * up
    rows = total.shape[0] // 2
    low = lax.broadcasted_iota(jnp.int32, (rows, 2 * hid), 1) < hid
    packed = jnp.where(low, value[:rows], pltpu.roll(value[rows:], hid, 1)).astype(bf16)
    for i in range(out_ref.shape[0]):
        out_ref[i] = packed


def down_body(h_ref, w_ref, after_ref, out_ref, wlo_ref, whi_ref):
    del after_ref
    count, rows, width = h_ref.shape
    hid = width // 2
    zero = jnp.zeros((hid, w_ref.shape[1]), bf16)
    for j in range(count):
        part = w_ref[hid * j : hid * (j + 1), :]
        wlo_ref[width * j : width * j + hid, :] = part
        wlo_ref[width * j + hid : width * (j + 1), :] = zero
        whi_ref[width * j : width * j + hid, :] = zero
        whi_ref[width * j + hid : width * (j + 1), :] = part
    top = bottom = None
    for j in range(0, count, 2):
        pair = jnp.concatenate([h_ref[j], h_ref[j + 1]], axis=1)
        a = dot(pair, wlo_ref[width * j : width * (j + 2), :])
        b = dot(pair, whi_ref[width * j : width * (j + 2), :])
        top = a if top is None else top + a
        bottom = b if bottom is None else bottom + b
    groups, both, width = out_ref.shape
    cap = both // 2
    out_ref[:, :cap, :] = top.reshape(groups, cap, width).astype(bf16)
    out_ref[:, cap:, :] = bottom.reshape(groups, cap, width).astype(bf16)


def routing_body(routes_ref, weight_ref, pick_ref, share_ref, *, experts, cap):
    top_k, rows = routes_ref.shape
    both = jnp.concatenate(
        [routes_ref[...].astype(f32), weight_ref[...], jnp.zeros((128 - 2 * top_k, rows), f32)],
        axis=0,
    ).T
    named = [both[:, k : k + 1].astype(jnp.int32) for k in range(top_k)]
    ids = lax.broadcasted_iota(jnp.int32, (rows, experts), 1)
    each = [(ids == name).astype(f32) for name in named]
    hits = each[0]
    total = both[:, top_k : top_k + 1]
    for k in range(1, top_k):
        hits = hits + each[k]
        total = total + both[:, top_k + k : top_k + k + 1]
    before = lax.broadcasted_iota(jnp.int32, (rows, rows), 1) < lax.broadcasted_iota(
        jnp.int32, (rows, rows), 0
    )
    rank = dot(before.astype(f32).astype(bf16), hits.astype(bf16))
    lane = lax.broadcasted_iota(jnp.int32, (rows, experts * cap), 1)
    for k in range(top_k):
        own_rank = jnp.sum(rank * each[k], axis=-1, keepdims=True).astype(jnp.int32)
        place = named[k] * cap + own_rank
        pick_ref[k] = (lane == place).astype(f32).astype(bf16)
        share = both[:, top_k + k : top_k + k + 1] / total
        share_ref[k] = jnp.broadcast_to(share, share_ref.shape[1:])


def combine_body(back_ref, pick_ref, share_ref, out_ref):
    back = back_ref[...]
    out = None
    for k in range(pick_ref.shape[0]):
        share = share_ref[k]
        share = jnp.concatenate([share] * (back.shape[1] // share.shape[1]), axis=1)
        term = dot(pick_ref[k], back) * share
        out = term if out is None else out + term
    out_ref[...] = out.astype(bf16)


def on_device(
    query_input,
    key_input,
    value_input,
    query_gain,
    key_gain,
    mixer_out,
    moe_input,
    moe_gain,
    routes,
    route_weight,
    expert_gate,
    expert_up,
    expert_down,
):
    seq, q_cols = query_input.shape
    hw = query_gain.shape[0]
    tokens, model = moe_input.shape
    tp = lax.axis_size(TP)
    ep = lax.axis_size(EP)
    ny = lax.axis_size("y")
    nx = lax.axis_size("x")
    width = model // tp
    experts = ep
    cap = 3 * tokens * routes.shape[1] // (2 * experts)
    slots = experts * cap
    hid = expert_gate.shape[2]

    at_y, at_x = lax.axis_index("y"), lax.axis_index("x")
    at_yx = jnp.stack([at_y, at_x]).astype(jnp.int32)
    smem = pl.BlockSpec(memory_space=pltpu.SMEM)
    vmem = pl.BlockSpec(memory_space=pltpu.VMEM)
    hbm = pl.BlockSpec(memory_space=pltpu.HBM)
    anywhere = pl.BlockSpec(memory_space=pl.ANY)

    positions = lax.axis_index(EP) * seq + jnp.arange(seq, dtype=jnp.int32)
    quarter = hw // 4
    inverse = BASE ** (-jnp.arange(quarter, dtype=f32) / quarter)
    row = (positions // GRID_W).astype(f32)
    col = (positions % GRID_W).astype(f32)
    angles = jnp.concatenate(
        [inverse[:, None] * row[None, :], inverse[:, None] * col[None, :]], axis=0
    )
    cos, sin = jnp.cos(angles), jnp.sin(angles)
    chunk = pl.pallas_call(
        key_body,
        out_shape=jax.ShapeDtypeStruct((seq, 2 * hw), bf16),
        in_specs=[hbm, hbm, hbm, vmem, vmem],
        scratch_shapes=[
            pltpu.VMEM((hw, seq), bf16),
            pltpu.VMEM((hw, seq), bf16),
            pltpu.VMEM((1, hw), f32),
            pltpu.SemaphoreType.DMA((3,)),
        ],
        compiler_params=params(60),
        name="keys",
    )(key_input.T, value_input.T, key_gain[None, :], cos, sin)
    keys = lax.all_gather(chunk, EP, axis=0, tiled=True)

    own = pl.pallas_call(
        lambda *refs: dispatch_body(*refs, experts=experts, cap=cap),
        out_shape=jax.ShapeDtypeStruct((slots, width), bf16),
        in_specs=[smem, hbm, hbm, hbm],
        scratch_shapes=[
            pltpu.VMEM((tokens, model), bf16),
            pltpu.VMEM((1, model), f32),
            pltpu.VMEM((routes.shape[1], tokens), jnp.int32),
            pltpu.SemaphoreType.DMA((3,)),
        ],
        compiler_params=params(60),
        name="dispatch",
    )(lax.axis_index(TP)[None].astype(jnp.int32), moe_input, moe_gain[None, :], routes.T)
    nz = lax.axis_size("z")
    received = lax.all_to_all(
        own.reshape(nz, 2 * cap, width), "z", split_axis=0, concat_axis=0, tiled=True
    )

    q_t = pl.pallas_call(
        query_body,
        out_shape=jax.ShapeDtypeStruct((hw, seq * q_cols // hw), bf16),
        compiler_params=params(),
        name="queries",
    )(query_input, query_gain[None, :], cos, sin)
    both = jnp.concatenate([expert_gate[0].T, expert_up[0].T], axis=0)
    deep = model // ny
    gate_up = []
    for d in range(ny):
        part = lax.dynamic_slice_in_dim(both, (at_y ^ d) * deep, deep, 1)
        if d:
            part = lax.ppermute(part, "y", [(i, i ^ d) for i in range(ny)])
        gate_up.append(part)
    pick, share = pl.pallas_call(
        lambda *refs: routing_body(*refs, experts=experts, cap=cap),
        out_shape=(
            jax.ShapeDtypeStruct((routes.shape[1], tokens, slots), bf16),
            jax.ShapeDtypeStruct((routes.shape[1], tokens, 128), f32),
        ),
        compiler_params=params(),
        name="routing",
    )(routes.T, route_weight.T)

    block = pl.pallas_call(
        spread_body,
        out_shape=jax.ShapeDtypeStruct((2 * nx, slots // 2, width), bf16),
        in_specs=[vmem] + [anywhere] * 5,
        compiler_params=params(),
        name="spread",
    )(received, *gate_up[1:], q_t, pick)
    block = lax.all_to_all(block, ("core", "x"), split_axis=0, concat_axis=0, tiled=True)
    rows_y = mixer_out.shape[0] // ny
    mixer = []
    for d in range(ny):
        part = lax.dynamic_slice_in_dim(mixer_out, (at_y ^ d) * rows_y, rows_y, 0)
        if d:
            part = lax.ppermute(part, "y", [(i, i ^ d) for i in range(ny)])
        mixer.append(part)

    partial = pl.pallas_call(
        gate_up_body,
        out_shape=jax.ShapeDtypeStruct((ny, slots, 2 * hid), bf16),
        in_specs=[smem] + [vmem] * 5 + [anywhere],
        compiler_params=params(),
        name="gate_up",
    )(at_yx, block, *gate_up, sum(part[:8, :128] for part in mixer[1:]))
    partial = lax.all_to_all(partial, "y", split_axis=0, concat_axis=0, tiled=True)
    hidden = pl.pallas_call(
        hidden_body,
        out_shape=jax.ShapeDtypeStruct((tp, slots // 2, 2 * hid), bf16),
        compiler_params=params(),
        name="hidden",
    )(partial)
    all_hidden = lax.all_to_all(hidden, TP, split_axis=0, concat_axis=0, tiled=True)

    step_rows = 4 * seq
    attended = pl.pallas_call(
        lambda *refs: attend_body(*refs, n=seq, hw=hw, tile=256),
        out_shape=jax.ShapeDtypeStruct((seq, q_cols), bf16),
        grid=(ep * seq // step_rows,),
        in_specs=[
            pl.BlockSpec(q_t.shape, lambda i: (0, 0)),
            pl.BlockSpec((step_rows, 2 * hw), lambda i: (i, 0)),
        ],
        out_specs=pl.BlockSpec((seq, q_cols), lambda i: (0, 0)),
        scratch_shapes=[
            pltpu.VMEM((2 * hw, q_t.shape[1]), bf16),
            pltpu.VMEM((2 * hw, q_t.shape[1]), bf16),
            pltpu.VMEM((1, q_t.shape[1]), f32),
            pltpu.VMEM((hw + 16, q_t.shape[1]), f32),
            pltpu.VMEM((2, seq, 256), f32),
            pltpu.VMEM((2, seq, 256), bf16),
        ],
        compiler_params=params(32),
        cost_estimate=pl.CostEstimate(
            flops=4 * seq * seq * ep * q_cols, bytes_accessed=4 << 20, transcendentals=0
        ),
        name="attend",
    )(q_t, keys)
    parts = [attended]
    for d in range(1, nx):
        parts.append(lax.ppermute(attended, "x", [(i, i ^ d) for i in range(nx)]))

    expert_out = pl.pallas_call(
        down_body,
        out_shape=jax.ShapeDtypeStruct((nz, 2 * cap, width), bf16),
        in_specs=[vmem, vmem, anywhere],
        scratch_shapes=[
            pltpu.VMEM((2 * hid * tp, width), bf16),
            pltpu.VMEM((2 * hid * tp, width), bf16),
        ],
        compiler_params=params(),
        name="down",
    )(all_hidden, expert_down[0], attended)
    returned = lax.all_to_all(
        expert_out.reshape(ep, cap, width), EP, split_axis=0, concat_axis=0, tiled=True
    ).reshape(slots, width)

    features = mixer_out.shape[1]
    turned = pl.pallas_call(
        weights_body,
        out_shape=jax.ShapeDtypeStruct((ny, rows_y, features), bf16),
        in_specs=[smem] + [vmem] * 4 + [anywhere],
        compiler_params=params(),
        name="weights",
    )(at_yx, *mixer, attended[:8, :])
    mixed = pl.pallas_call(
        mixer_body,
        out_shape=[jax.ShapeDtypeStruct((seq, features), f32)]
        + [jax.ShapeDtypeStruct((seq, features), bf16)] * (ny - 1),
        compiler_params=params(),
        name="mixer",
    )(*parts, turned)
    sums = [mixed[0]]
    for d in range(1, ny):
        sums.append(lax.ppermute(mixed[d], "y", [(i, i ^ d) for i in range(ny)]))
    attn_mixed = pl.pallas_call(
        mixed_body,
        out_shape=jax.ShapeDtypeStruct((seq, features), bf16),
        compiler_params=params(),
        name="mixed",
    )(*sums)

    moe_out = pl.pallas_call(
        combine_body,
        out_shape=jax.ShapeDtypeStruct((tokens, width), bf16),
        compiler_params=params(),
        name="combine",
    )(returned, pick, share)
    return (attn_mixed, moe_out)


def solution(mesh):
    torus = Mesh(mesh.devices.reshape(mesh.shape["ep"] // 2, 2, 4, 4), (*EP, *TP))
    placed = (
        P(EP, TP),
        P(EP, TP),
        P(EP, TP),
        P(),
        P(),
        P(None, TP),
        P(EP, None),
        P(),
        P(EP, None),
        P(EP, None),
        P(EP, None, TP),
        P(EP, None, TP),
        P(EP, None, TP),
    )
    return jax.shard_map(
        on_device,
        mesh=torus,
        in_specs=placed,
        out_specs=(P(EP, TP), P(EP, TP)),
        check_vma=False,
    )
```

time: 331 us -> 194 us (0.59)
  matrix products: 71.3 us -> 0 us
  local copies, waits for them, and re-layouts: 71.6 us -> 8.31 us
  waiting for transfers between devices: 85.6 us -> 36.7 us
  starting transfers between devices: 33 us -> 76.9 us
  Pallas kernels: 0 us -> 40.7 us
  other arithmetic: 22.3 us -> 1.16 us
  blocking collectives: 29.6 us -> 14.3 us
    dot_general x68 -> x0, matrix products: 71.3 us -> none  [the longest x32 43.9 us: one_block(): jnp.einsum('qkgd,skd->kgqs', query_rot, key_block[:, 0], preferred_elemen...]
    all_to_all x3 -> x4, waiting for transfers between devices: 46.2 us -> 0.01 us  [the longest x1 0.01 us: on_device(): lax.all_to_all(block, ('core', 'x'), split_axis=0, concat_axis=0, tiled=T...]
    pallas_call x0 -> x13, Pallas kernels: none -> 40.7 us  [the longest x1 24.3 us: on_device(): pl.pallas_call(lambda *refs: attend_body(*refs, n=seq, hw=hw, tile=256),...]
    all_gather x3 -> x1, waiting for transfers between devices: 39.4 us -> 0.02 us  [on_device(): keys = lax.all_gather(chunk, EP, axis=0, tiled=True)]
    ppermute x0 -> x12, starting transfers between devices: none -> 38.1 us  [the longest x6 19.4 us: on_device(): part = lax.ppermute(part, 'y', [(i, i ^ d) for i in range(ny)])]
    ppermute x0 -> x12, waiting for transfers between devices: none -> 36.6 us  [the longest x6 22.3 us: on_device(): part = lax.ppermute(part, 'y', [(i, i ^ d) for i in range(ny)])]
    all_gather x1 -> x0, blocking collectives: 29.6 us -> none  [gather_axes(): x = lax.all_gather(x, axis, axis=dim, tiled=True)]
    squeeze x32 -> x0, local copies, waits for them, and re-layouts: 29.4 us -> none  [on_device(): current, _ = lax.scan(one_block, initial, key_blocks)]
  transfers between devices with their start and end apart: 6 -> 17, of which waited for: 4 -> 9; matrix products, arithmetic and copies ran while one was open for 43% -> 1% of each run, Pallas kernels for 0% -> 18%
where the time goes in v1:
time: 194 us; the launch traced here: 193 us
  starting transfers between devices  76.9 us (40%)
  Pallas kernels  40.7 us (21%)
  waiting for transfers between devices  36.7 us (19%)
  between operations  14.5 us (7%)
  blocking collectives  14.3 us (7%)
  local copies, waits for them, and re-layouts  8.31 us (4%)
    pallas_call x1, Pallas kernels, on_device(): pl.pallas_call(lambda *refs: attend_body(*refs, n=seq, hw=hw, tile=256),...  24.3 us
    ppermute x6, waiting for transfers between devices, on_device(): part = lax.ppermute(part, 'y', [(i, i ^ d) for i in range(ny)])  22.3 us
    ppermute x6, starting transfers between devices, on_device(): part = lax.ppermute(part, 'y', [(i, i ^ d) for i in range(ny)])  19.4 us
    all_to_all x1, starting transfers between devices, on_device(): lax.all_to_all(own.reshape(nz, 2 * cap, width), 'z', split_axis=0, concat...  15.9 us
    all_to_all x1, blocking collectives, on_device(): lax.all_to_all(partial, 'y', split_axis=0, concat_axis=0, tiled=True)  14.3 us
    ppermute x3, waiting for transfers between devices, on_device(): sums.append(lax.ppermute(mixed[d], 'y', [(i, i ^ d) for i in range(ny)]))  12.6 us
    ppermute x3, starting transfers between devices, on_device(): sums.append(lax.ppermute(mixed[d], 'y', [(i, i ^ d) for i in range(ny)]))  9.58 us
    all_to_all x1, starting transfers between devices, on_device(): lax.all_to_all(expert_out.reshape(ep, cap, width), EP, split_axis=0, conc...  9.36 us
  transfers between devices with their start and end apart: 17, of which 9 were waited for; matrix products, arithmetic and copies ran while one was open for 1% of the time, Pallas kernels for 18%

profile of v1, /device:TPU:1, one launch (start us, length us, event | category | flops | bytes accessed | tf_op | source)
XLA Modules:
  0.0 192.5 jit_solution(2050380758855352616)
XLA Ops:
  7.3 0.9 fusion.4
  8.2 2.6 %keys.1 = bf16[512,128]{1,0:T(8,128)(2,1)} custom-call(bf16[64,512]{1,0:T(8,128)(2,1)} %bitcast.29, bf16[64,512]{1,0:T(8,128)(2,1)} %bitcast.30, f32[1,64]{1,0:T(1,128)} %bitcast.32, f32[32,512]{1,0:T(8,128)} %get-tuple-element.23.cos_ref, f32[32,512]{1,0:T(8,128)} %get-tuple-element.22.sin_ref), custom_call_target="tpu_custom_call" | custom-call | tf_op jit(solution)/shard_map/keys/pallas_call | solution.py:355
  10.9 3.3 %dispatch.1 = bf16[768,256]{1,0:T(8,128)(2,1)} custom-call(s32[1]{0:T(128)} %bitcast.6.refs_0_, bf16[256,4096]{1,0:T(8,128)(2,1)} %refs_1_.1, f32[1,4096]{1,0:T(1,128)} %bitcast.31, s32[2,256]{1,0:T(2,128)} %bitcast.22), custom_call_target="tpu_custom_call" | custom-call | tf_op jit(solution)/shard_map/dispatch/pallas_call | solution.py:370
  14.2 15.9 %all-to-all-start = ((bf16[16,48,256]{2,1,0:T(8,128)(2,1)}), bf16[16,48,256]{2,1,0:T(8,128)(2,1)S(1)}, u32[]{:S(2)}, u32[]{:S(2)}) async-start(bf16[16,48,256]{2,1,0:T(8,128)(2,1)} %bitcast.26), calls=%async_computation | async-start | bytes 786432 | tf_op jit(solution)/shard_map/all_to_all | solution.py:384
  30.2 0.1 fusion
  30.3 3.2 %collective-permute-start.9 = (bf16[128,1024]{1,0:T(8,128)(2,1)S(1)}, bf16[128,1024]{1,0:T(8,128)(2,1)S(1)}, u32[]{:S(2)}, u32[]{:S(2)}) collective-permute-start(bf16[128,1024]{1,0:T(8,128)(2,1)S(1)} %get-tuple-element.15), channel_id=1, source_target_pairs={{0,4},{4,0},{8,12},{12,8},{1,5},{5,1},{9,13},{13,9},{2,6},{6,2},{1... | collective-permute-start | bytes 786440 | tf_op jit(solution)/shard_map/ppermute | solution.py:400
  33.5 4.5 %collective-permute-start.10 = (bf16[128,1024]{1,0:T(8,128)(2,1)S(1)}, bf16[128,1024]{1,0:T(8,128)(2,1)S(1)}, u32[]{:S(2)}, u32[]{:S(2)}) collective-permute-start(bf16[128,1024]{1,0:T(8,128)(2,1)S(1)} %get-tuple-element.16), channel_id=1, source_target_pairs={{0,8},{4,12},{8,0},{12,4},{1,9},{5,13},{9,1},{13,5},{2,10},{6,14},... | collective-permute-start | bytes 786440 | tf_op jit(solution)/shard_map/ppermute | solution.py:400
  38.0 1.9 collective-permute-start.11
  40.0 1.0 routing.1
  41.0 0.2 queries.1.refs_0_.refs_3_
  41.2 6.0 %collective-permute-done.10.refs_1_.w2_ref = bf16[128,1024]{1,0:T(8,128)(2,1)S(1)} collective-permute-done((bf16[128,1024]{1,0:T(8,128)(2,1)S(1)}, bf16[128,1024]{1,0:T(8,128)(2,1)S(1)}, u32[]{:S(2)}, u32[]{:S(2)}) %collective-permute-start.10) | collective-permute-done | bytes 262176 | tf_op jit(solution)/shard_map/ppermute | solution.py:400
  47.2 6.5 %collective-permute-done.11.refs_2_.w3_ref = bf16[128,1024]{1,0:T(8,128)(2,1)S(1)} collective-permute-done((bf16[128,1024]{1,0:T(8,128)(2,1)S(1)}, bf16[128,1024]{1,0:T(8,128)(2,1)S(1)}, u32[]{:S(2)}, u32[]{:S(2)}) %collective-permute-start.11) | collective-permute-done | bytes 262176 | tf_op jit(solution)/shard_map/ppermute | solution.py:400
  53.7 1.3 spread.1
  55.0 9.2 %all-to-all-start.1 = ((bf16[8,384,256]{2,1,0:T(8,128)(2,1)}), bf16[8,384,256]{2,1,0:T(8,128)(2,1)S(1)}, u32[]{:S(2)}, u32[]{:S(2)}) async-start(bf16[8,384,256]{2,1,0:T(8,128)(2,1)} %spread.1), calls=%async_computation.1 | async-start | bytes 3145728 | tf_op jit(solution)/shard_map/all_to_all | solution.py:419
  64.2 2.0 %constant_dynamic-slice_fusion = (bf16[512,256]{1,0:T(8,128)(2,1)S(1)}, bf16[512,256]{1,0:T(8,128)(2,1)S(1)}, bf16[512,256]{1,0:T(8,128)(2,1)}, bf16[512,256]{1,0:T(8,128)(2,1)S(1)}) fusion(bf16[2048,256]{1,0:T(8,128)(2,1)} %param.18, s32[]{:T(128)S(6)} %select_n.49, s32[]{:T(128)S(6)} %select_n.47, s32[]{:T(128)S(6)} %select_n.46, s32[]{:T(128)S(6)} %select_n.48), kind=kLoop, calls=%fused_computation.22 | loop fusion | bytes 2097168 | tf_op jit(solution)/shard_map/dynamic_slice | solution.py:423
  66.1 4.7 %collective-permute-start.5 = (bf16[512,256]{1,0:T(8,128)(2,1)S(1)}, bf16[512,256]{1,0:T(8,128)(2,1)S(1)}, u32[]{:S(2)}, u32[]{:S(2)}) collective-permute-start(bf16[512,256]{1,0:T(8,128)(2,1)S(1)} %get-tuple-element.18), channel_id=1, source_target_pairs={{0,12},{4,8},{8,4},{12,0},{1,13},{5,9},{9,5},{13,1},{2,14},{6,10},... | collective-permute-start | bytes 786440 | tf_op jit(solution)/shard_map/ppermute | solution.py:425
  70.8 1.9 collective-permute-start.3
  72.8 3.1 %collective-permute-start.4 = (bf16[512,256]{1,0:T(8,128)(2,1)S(1)}, bf16[512,256]{1,0:T(8,128)(2,1)S(1)}, u32[]{:S(2)}, u32[]{:S(2)}) collective-permute-start(bf16[512,256]{1,0:T(8,128)(2,1)S(1)} %get-tuple-element.21), channel_id=1, source_target_pairs={{0,8},{4,12},{8,0},{12,4},{1,9},{5,13},{9,1},{13,5},{2,10},{6,14},... | collective-permute-start | bytes 786440 | tf_op jit(solution)/shard_map/ppermute | solution.py:425
  75.9 1.5 collective-permute-done.5.w3
  77.5 2.9 %collective-permute-done.3.w1 = bf16[512,256]{1,0:T(8,128)(2,1)S(1)} collective-permute-done((bf16[512,256]{1,0:T(8,128)(2,1)S(1)}, bf16[512,256]{1,0:T(8,128)(2,1)S(1)}, u32[]{:S(2)}, u32[]{:S(2)}) %collective-permute-start.3) | collective-permute-done | bytes 262176 | tf_op jit(solution)/shard_map/ppermute | solution.py:425
  80.4 5.4 %collective-permute-done.4.w2 = bf16[512,256]{1,0:T(8,128)(2,1)S(1)} collective-permute-done((bf16[512,256]{1,0:T(8,128)(2,1)S(1)}, bf16[512,256]{1,0:T(8,128)(2,1)S(1)}, u32[]{:S(2)}, u32[]{:S(2)}) %collective-permute-start.4) | collective-permute-done | bytes 262176 | tf_op jit(solution)/shard_map/ppermute | solution.py:425
  85.8 0.7 copy-done.4
  86.5 0.7 copy-done.6
  87.3 0.7 copy-done.8
  88.0 1.6 gate_up.1
  89.6 14.3 %all_to_all.25.parts_ref = bf16[4,768,128]{2,1,0:T(8,128)(2,1)S(1)} all-to-all(bf16[4,768,128]{2,1,0:T(8,128)(2,1)S(1)} %gate_up.1), channel_id=1, replica_groups=mesh['z'=16,'core'=2,'y'=4,'x'=4] {'y'}, dimensions={0} | all-to-all | bytes 1572864 | tf_op jit(solution)/shard_map/all_to_all | solution.py:435
  103.8 1.6 hidden.1
  105.4 4.3 %all-to-all-start.3 = ((bf16[16,384,128]{2,1,0:T(8,128)(2,1)}), bf16[16,384,128]{2,1,0:T(8,128)(2,1)S(1)}, u32[]{:S(2)}, u32[]{:S(2)}) async-start(bf16[16,384,128]{2,1,0:T(8,128)(2,1)} %hidden.1), calls=%async_computation.3 | async-start | bytes 3145728 | tf_op jit(solution)/shard_map/all_to_all | solution.py:442
  109.8 2.2 %copy-done.16 = bf16[16384,128]{1,0:T(8,128)(2,1)S(1)} copy-done((bf16[16384,128]{1,0:T(8,128)(2,1)S(1)}, bf16[16384,128]{1,0:T(8,128)(2,1)}, u32[]{:S(2)}) %copy-start.16) | copy-done | bytes 4194328
  112.0 24.3 %attend.1.a0.after_ref = bf16[512,128]{1,0:T(8,128)(2,1)S(1)} custom-call(bf16[64,1024]{1,0:T(8,128)(2,1)S(1)} %queries.1.refs_0_.refs_3_, bf16[16384,128]{1,0:T(8,128)(2,1)S(1)} %copy-done.16), custom_call_target="tpu_custom_call" | custom-call | flops 4294967296 | bytes 4194304 | tf_op jit(solution)/shard_map/attend/pallas_call | solution.py:445
  136.3 1.7 down.1
  138.1 9.4 %all-to-all-start.4 = ((bf16[32,24,256]{2,1,0:T(8,128)(2,1)}), bf16[32,24,256]{2,1,0:T(8,128)(2,1)S(1)}, u32[]{:S(2)}, u32[]{:S(2)}) async-start(bf16[32,24,256]{2,1,0:T(8,128)(2,1)} %bitcast.16), calls=%async_computation.4 | async-start | bytes 786432 | tf_op jit(solution)/shard_map/all_to_all | solution.py:483
  147.4 4.8 %collective-permute-start.2 = (bf16[512,128]{1,0:T(8,128)(2,1)S(1)}, bf16[512,128]{1,0:T(8,128)(2,1)S(1)}, u32[]{:S(2)}, u32[]{:S(2)}) collective-permute-start(bf16[512,128]{1,0:T(8,128)(2,1)S(1)} %attend.1.a0.after_ref), channel_id=1, source_target_pairs={{0,3},{1,2},{2,1},{3,0},{4,7},{5,6},{6,5},{7,4},{8,11},{9,10},{10,... | collective-permute-start | bytes 393224 | tf_op jit(solution)/shard_map/ppermute | solution.py:470
  152.2 2.5 %collective-permute-start.1 = (bf16[512,128]{1,0:T(8,128)(2,1)S(1)}, bf16[512,128]{1,0:T(8,128)(2,1)S(1)}, u32[]{:S(2)}, u32[]{:S(2)}) collective-permute-start(bf16[512,128]{1,0:T(8,128)(2,1)S(1)} %attend.1.a0.after_ref), channel_id=1, source_target_pairs={{0,2},{1,3},{2,0},{3,1},{4,6},{5,7},{6,4},{7,5},{8,10},{9,11},{10,... | collective-permute-start | bytes 393224 | tf_op jit(solution)/shard_map/ppermute | solution.py:470
  154.7 1.9 collective-permute-start
  156.7 0.9 copy-done.7
  157.6 0.9 copy-done.9
  158.6 0.6 weights.1.w_ref
  159.2 0.9 collective-permute-done.1.a2
  160.1 0.7 collective-permute-done.a1
  160.8 0.7 mixer.1
  161.6 3.1 %collective-permute-start.6 = (bf16[512,256]{1,0:T(8,128)(2,1)S(1)}, bf16[512,256]{1,0:T(8,128)(2,1)S(1)}, u32[]{:S(2)}, u32[]{:S(2)}) collective-permute-start(bf16[512,256]{1,0:T(8,128)(2,1)S(1)} %get-tuple-element.9), channel_id=1, source_target_pairs={{0,4},{4,0},{8,12},{12,8},{1,5},{5,1},{9,13},{13,9},{2,6},{6,2},{1... | collective-permute-start | bytes 786440 | tf_op jit(solution)/shard_map/ppermute | solution.py:504
  164.7 4.3 %collective-permute-start.7 = (bf16[512,256]{1,0:T(8,128)(2,1)S(1)}, bf16[512,256]{1,0:T(8,128)(2,1)S(1)}, u32[]{:S(2)}, u32[]{:S(2)}) collective-permute-start(bf16[512,256]{1,0:T(8,128)(2,1)S(1)} %get-tuple-element.10), channel_id=1, source_target_pairs={{0,8},{4,12},{8,0},{12,4},{1,9},{5,13},{9,1},{13,5},{2,10},{6,14},... | collective-permute-start | bytes 786440 | tf_op jit(solution)/shard_map/ppermute | solution.py:504
  169.0 2.2 %collective-permute-start.8 = (bf16[512,256]{1,0:T(8,128)(2,1)S(1)}, bf16[512,256]{1,0:T(8,128)(2,1)S(1)}, u32[]{:S(2)}, u32[]{:S(2)}) collective-permute-start(bf16[512,256]{1,0:T(8,128)(2,1)S(1)} %get-tuple-element.11), channel_id=1, source_target_pairs={{0,12},{4,8},{8,4},{12,0},{1,13},{5,9},{9,5},{13,1},{2,14},{6,10},... | collective-permute-start | bytes 786440 | tf_op jit(solution)/shard_map/ppermute | solution.py:504
  171.2 6.3 %collective-permute-done.7.r2_ref = bf16[512,256]{1,0:T(8,128)(2,1)S(1)} collective-permute-done((bf16[512,256]{1,0:T(8,128)(2,1)S(1)}, bf16[512,256]{1,0:T(8,128)(2,1)S(1)}, u32[]{:S(2)}, u32[]{:S(2)}) %collective-permute-start.7) | collective-permute-done | bytes 262176 | tf_op jit(solution)/shard_map/ppermute | solution.py:504
  177.4 6.4 %collective-permute-done.8.r3_ref = bf16[512,256]{1,0:T(8,128)(2,1)S(1)} collective-permute-done((bf16[512,256]{1,0:T(8,128)(2,1)S(1)}, bf16[512,256]{1,0:T(8,128)(2,1)S(1)}, u32[]{:S(2)}, u32[]{:S(2)}) %collective-permute-start.8) | collective-permute-done | bytes 262176 | tf_op jit(solution)/shard_map/ppermute | solution.py:504
  183.8 0.8 mixed.1
  184.6 1.0 combine.1
  (48 shorter events, 0.4 us)
Async XLA Ops:
  7.2 102.6 %all-gather.2.cloned.1.call-start = ((), (), s32[]{:S(2)}) async-start(), calls=%async_computation.5 | async-start | bytes 4325376 | tf_op jit(solution)/shard_map/all_gather | solution.py:368
  10.9 19.3 %copy-start.17 = (bf16[1,4096,64]{1,2,0:T(8,128)(2,1)S(1)}, bf16[1,4096,64]{1,2,0:T(8,128)(2,1)}, u32[]{:S(2)}) copy-start(bf16[1,4096,64]{1,2,0:T(8,128)(2,1)} %param.23) | copy-start | bytes 1572868
  10.9 19.3 %copy-start.18 = (bf16[1,4096,64]{1,2,0:T(8,128)(2,1)S(1)}, bf16[1,4096,64]{1,2,0:T(8,128)(2,1)}, u32[]{:S(2)}) copy-start(bf16[1,4096,64]{1,2,0:T(8,128)(2,1)} %param.24) | copy-start | bytes 1572868
  14.2 25.8 %copy-start.13 = (s32[256,2]{0,1:T(2,128)S(1)}, s32[256,2]{0,1:T(2,128)}, u32[]{:S(2)}) copy-start(s32[256,2]{0,1:T(2,128)} %param.21) | copy-start | bytes 6148
  14.2 25.8 %copy-start.14 = (f32[256,2]{0,1:T(2,128)S(1)}, f32[256,2]{0,1:T(2,128)}, u32[]{:S(2)}) copy-start(f32[256,2]{0,1:T(2,128)} %param.22) | copy-start | bytes 6148
  14.2 26.7 %copy-start.1 = (f32[32,512]{1,0:T(8,128)S(1)}, f32[32,512]{1,0:T(8,128)}, u32[]{:S(2)}) copy-start(f32[32,512]{1,0:T(8,128)} %get-tuple-element.22.sin_ref) | copy-start | bytes 196612
  14.2 26.7 %copy-start.2 = (f32[32,512]{1,0:T(8,128)S(1)}, f32[32,512]{1,0:T(8,128)}, u32[]{:S(2)}) copy-start(f32[32,512]{1,0:T(8,128)} %get-tuple-element.23.cos_ref) | copy-start | bytes 196612
  14.2 26.7 %copy-start.12 = (bf16[512,128]{1,0:T(8,128)(2,1)S(1)}, bf16[512,128]{1,0:T(8,128)(2,1)}, u32[]{:S(2)}) copy-start(bf16[512,128]{1,0:T(8,128)(2,1)} %q_ref.1) | copy-start | bytes 393220
  14.2 26.7 %copy-start.15 = (f32[64]{0:T(128)S(1)}, f32[64]{0:T(128)}, u32[]{:S(2)}) copy-start(f32[64]{0:T(128)} %param.16) | copy-start | bytes 772
  14.2 39.4 %all-to-all-start = ((bf16[16,48,256]{2,1,0:T(8,128)(2,1)}), bf16[16,48,256]{2,1,0:T(8,128)(2,1)S(1)}, u32[]{:S(2)}, u32[]{:S(2)}) async-start(bf16[16,48,256]{2,1,0:T(8,128)(2,1)} %bitcast.26), calls=%async_computation | async-start | bytes 786432 | tf_op jit(solution)/shard_map/all_to_all | solution.py:384
  30.3 10.9 %collective-permute-start.9 = (bf16[128,1024]{1,0:T(8,128)(2,1)S(1)}, bf16[128,1024]{1,0:T(8,128)(2,1)S(1)}, u32[]{:S(2)}, u32[]{:S(2)}) collective-permute-start(bf16[128,1024]{1,0:T(8,128)(2,1)S(1)} %get-tuple-element.15), channel_id=1, source_target_pairs={{0,4},{4,0},{8,12},{12,8},{1,5},{5,1},{9,13},{13,9},{2,6},{6,2},{1... | collective-permute-start | bytes 786440 | tf_op jit(solution)/shard_map/ppermute | solution.py:400
  33.5 13.7 %collective-permute-start.10 = (bf16[128,1024]{1,0:T(8,128)(2,1)S(1)}, bf16[128,1024]{1,0:T(8,128)(2,1)S(1)}, u32[]{:S(2)}, u32[]{:S(2)}) collective-permute-start(bf16[128,1024]{1,0:T(8,128)(2,1)S(1)} %get-tuple-element.16), channel_id=1, source_target_pairs={{0,8},{4,12},{8,0},{12,4},{1,9},{5,13},{9,1},{13,5},{2,10},{6,14},... | collective-permute-start | bytes 786440 | tf_op jit(solution)/shard_map/ppermute | solution.py:400
  38.0 15.6 %collective-permute-start.11 = (bf16[128,1024]{1,0:T(8,128)(2,1)S(1)}, bf16[128,1024]{1,0:T(8,128)(2,1)S(1)}, u32[]{:S(2)}, u32[]{:S(2)}) collective-permute-start(bf16[128,1024]{1,0:T(8,128)(2,1)S(1)} %get-tuple-element.17), channel_id=1, source_target_pairs={{0,12},{4,8},{8,4},{12,0},{1,13},{5,9},{9,5},{13,1},{2,14},{6,10},... | collective-permute-start | bytes 786440 | tf_op jit(solution)/shard_map/ppermute | solution.py:400
  40.9 14.0 %copy-start.10 = (f32[2,256,128]{2,1,0:T(8,128)}, f32[2,256,128]{2,1,0:T(8,128)S(1)}, u32[]{:S(2)}) copy-start(f32[2,256,128]{2,1,0:T(8,128)S(1)} %get-tuple-element.13.share_ref) | copy-start | bytes 786436
  55.0 33.0 %all-to-all-start.1 = ((bf16[8,384,256]{2,1,0:T(8,128)(2,1)}), bf16[8,384,256]{2,1,0:T(8,128)(2,1)S(1)}, u32[]{:S(2)}, u32[]{:S(2)}) async-start(bf16[8,384,256]{2,1,0:T(8,128)(2,1)} %spread.1), calls=%async_computation.1 | async-start | bytes 3145728 | tf_op jit(solution)/shard_map/all_to_all | solution.py:419
  66.1 11.4 %collective-permute-start.5 = (bf16[512,256]{1,0:T(8,128)(2,1)S(1)}, bf16[512,256]{1,0:T(8,128)(2,1)S(1)}, u32[]{:S(2)}, u32[]{:S(2)}) collective-permute-start(bf16[512,256]{1,0:T(8,128)(2,1)S(1)} %get-tuple-element.18), channel_id=1, source_target_pairs={{0,12},{4,8},{8,4},{12,0},{1,13},{5,9},{9,5},{13,1},{2,14},{6,10},... | collective-permute-start | bytes 786440 | tf_op jit(solution)/shard_map/ppermute | solution.py:425
  70.8 9.6 %collective-permute-start.3 = (bf16[512,256]{1,0:T(8,128)(2,1)S(1)}, bf16[512,256]{1,0:T(8,128)(2,1)S(1)}, u32[]{:S(2)}, u32[]{:S(2)}) collective-permute-start(bf16[512,256]{1,0:T(8,128)(2,1)S(1)} %get-tuple-element.19), channel_id=1, source_target_pairs={{0,4},{4,0},{8,12},{12,8},{1,5},{5,1},{9,13},{13,9},{2,6},{6,2},{1... | collective-permute-start | bytes 786440 | tf_op jit(solution)/shard_map/ppermute | solution.py:425
  72.8 13.0 %collective-permute-start.4 = (bf16[512,256]{1,0:T(8,128)(2,1)S(1)}, bf16[512,256]{1,0:T(8,128)(2,1)S(1)}, u32[]{:S(2)}, u32[]{:S(2)}) collective-permute-start(bf16[512,256]{1,0:T(8,128)(2,1)S(1)} %get-tuple-element.21), channel_id=1, source_target_pairs={{0,8},{4,12},{8,0},{12,4},{1,9},{5,13},{9,1},{13,5},{2,10},{6,14},... | collective-permute-start | bytes 786440 | tf_op jit(solution)/shard_map/ppermute | solution.py:425
  85.8 0.7 copy-start.4
  86.5 0.7 copy-start.6
  87.3 0.7 copy-start.8
  105.4 30.9 %all-to-all-start.3 = ((bf16[16,384,128]{2,1,0:T(8,128)(2,1)}), bf16[16,384,128]{2,1,0:T(8,128)(2,1)S(1)}, u32[]{:S(2)}, u32[]{:S(2)}) async-start(bf16[16,384,128]{2,1,0:T(8,128)(2,1)} %hidden.1), calls=%async_computation.3 | async-start | bytes 3145728 | tf_op jit(solution)/shard_map/all_to_all | solution.py:442
  109.7 26.6 %copy-start.3 = (bf16[1,1024,256]{2,1,0:T(8,128)(2,1)S(1)}, bf16[1,1024,256]{2,1,0:T(8,128)(2,1)}, u32[]{:S(2)}) copy-start(bf16[1,1024,256]{2,1,0:T(8,128)(2,1)} %param.25) | copy-start | bytes 1572868
  109.8 2.2 %copy-start.16 = (bf16[16384,128]{1,0:T(8,128)(2,1)S(1)}, bf16[16384,128]{1,0:T(8,128)(2,1)}, u32[]{:S(2)}) copy-start(bf16[16384,128]{1,0:T(8,128)(2,1)} %all-gather.2.cloned.1.call-done.refs_1_) | copy-start | bytes 12582916
  136.3 20.3 %copy-start = (bf16[512,256]{1,0:T(8,128)(2,1)S(1)}, bf16[512,256]{1,0:T(8,128)(2,1)}, u32[]{:S(2)}) copy-start(bf16[512,256]{1,0:T(8,128)(2,1)} %get-tuple-element.20.w0) | copy-start | bytes 786436
  136.3 20.3 %copy-start.5 = (bf16[512,256]{1,0:T(8,128)(2,1)S(1)}, bf16[512,256]{1,0:T(8,128)(2,1)}, u32[]{:S(2)}) copy-start(bf16[512,256]{1,0:T(8,128)(2,1)} %copy-done.4) | copy-start | bytes 786436
  138.1 46.6 %all-to-all-start.4 = ((bf16[32,24,256]{2,1,0:T(8,128)(2,1)}), bf16[32,24,256]{2,1,0:T(8,128)(2,1)S(1)}, u32[]{:S(2)}, u32[]{:S(2)}) async-start(bf16[32,24,256]{2,1,0:T(8,128)(2,1)} %bitcast.16), calls=%async_computation.4 | async-start | bytes 786432 | tf_op jit(solution)/shard_map/all_to_all | solution.py:483
  147.4 11.8 %collective-permute-start.2 = (bf16[512,128]{1,0:T(8,128)(2,1)S(1)}, bf16[512,128]{1,0:T(8,128)(2,1)S(1)}, u32[]{:S(2)}, u32[]{:S(2)}) collective-permute-start(bf16[512,128]{1,0:T(8,128)(2,1)S(1)} %attend.1.a0.after_ref), channel_id=1, source_target_pairs={{0,3},{1,2},{2,1},{3,0},{4,7},{5,6},{6,5},{7,4},{8,11},{9,10},{10,... | collective-permute-start | bytes 393224 | tf_op jit(solution)/shard_map/ppermute | solution.py:470
  152.2 7.9 %collective-permute-start.1 = (bf16[512,128]{1,0:T(8,128)(2,1)S(1)}, bf16[512,128]{1,0:T(8,128)(2,1)S(1)}, u32[]{:S(2)}, u32[]{:S(2)}) collective-permute-start(bf16[512,128]{1,0:T(8,128)(2,1)S(1)} %attend.1.a0.after_ref), channel_id=1, source_target_pairs={{0,2},{1,3},{2,0},{3,1},{4,6},{5,7},{6,4},{7,5},{8,10},{9,11},{10,... | collective-permute-start | bytes 393224 | tf_op jit(solution)/shard_map/ppermute | solution.py:470
  154.7 6.1 %collective-permute-start = (bf16[512,128]{1,0:T(8,128)(2,1)S(1)}, bf16[512,128]{1,0:T(8,128)(2,1)S(1)}, u32[]{:S(2)}, u32[]{:S(2)}) collective-permute-start(bf16[512,128]{1,0:T(8,128)(2,1)S(1)} %attend.1.a0.after_ref), channel_id=1, source_target_pairs={{0,1},{1,0},{2,3},{3,2},{4,5},{5,4},{6,7},{7,6},{8,9},{9,8},{10,11... | collective-permute-start | bytes 393224 | tf_op jit(solution)/shard_map/ppermute | solution.py:470
  156.7 1.0 copy-start.7
  157.6 0.9 copy-start.9
  159.2 25.5 %copy-start.11 = (f32[2,256,128]{2,1,0:T(8,128)S(1)}, f32[2,256,128]{2,1,0:T(8,128)}, u32[]{:S(2)}) copy-start(f32[2,256,128]{2,1,0:T(8,128)} %copy-done.10) | copy-start | bytes 786436
  161.6 9.6 %collective-permute-start.6 = (bf16[512,256]{1,0:T(8,128)(2,1)S(1)}, bf16[512,256]{1,0:T(8,128)(2,1)S(1)}, u32[]{:S(2)}, u32[]{:S(2)}) collective-permute-start(bf16[512,256]{1,0:T(8,128)(2,1)S(1)} %get-tuple-element.9), channel_id=1, source_target_pairs={{0,4},{4,0},{8,12},{12,8},{1,5},{5,1},{9,13},{13,9},{2,6},{6,2},{1... | collective-permute-start | bytes 786440 | tf_op jit(solution)/shard_map/ppermute | solution.py:504
  164.7 12.8 %collective-permute-start.7 = (bf16[512,256]{1,0:T(8,128)(2,1)S(1)}, bf16[512,256]{1,0:T(8,128)(2,1)S(1)}, u32[]{:S(2)}, u32[]{:S(2)}) collective-permute-start(bf16[512,256]{1,0:T(8,128)(2,1)S(1)} %get-tuple-element.10), channel_id=1, source_target_pairs={{0,8},{4,12},{8,0},{12,4},{1,9},{5,13},{9,1},{13,5},{2,10},{6,14},... | collective-permute-start | bytes 786440 | tf_op jit(solution)/shard_map/ppermute | solution.py:504
  169.0 14.8 %collective-permute-start.8 = (bf16[512,256]{1,0:T(8,128)(2,1)S(1)}, bf16[512,256]{1,0:T(8,128)(2,1)S(1)}, u32[]{:S(2)}, u32[]{:S(2)}) collective-permute-start(bf16[512,256]{1,0:T(8,128)(2,1)S(1)} %get-tuple-element.11), channel_id=1, source_target_pairs={{0,12},{4,8},{8,4},{12,0},{1,13},{5,9},{9,5},{13,1},{2,14},{6,10},... | collective-permute-start | bytes 786440 | tf_op jit(solution)/shard_map/ppermute | solution.py:504
Sparse Core Ops, SparseCore 0:
  11.0 88.4 all-gather.1

commit v2 on v1

--- a/solution.py
+++ b/solution.py
@@ -5,6 +5,7 @@
 from jax.experimental.pallas import tpu as pltpu
 from jax.sharding import Mesh
 from jax.sharding import PartitionSpec as P
+
 
 GRID_W = 64
 EP = ("z", "core")
@@ -82,10 +83,13 @@
     @pl.when(step == 0)
     def _():
         zero = jnp.zeros((hw, cols), bf16)
-        qlo_ref[:hw, :] = qt_ref[...]
-        qlo_ref[hw:, :] = zero
-        qhi_ref[:hw, :] = zero
-        qhi_ref[hw:, :] = qt_ref[...]
+        scaled = qt_ref[...].astype(f32) * LOG2E
+        big = scaled.astype(bf16)
+        small = (scaled - big.astype(f32)).astype(bf16)
+        for place, part in enumerate((big, zero, small, zero)):
+            qlo_ref[hw * place : hw * (place + 1), :] = part
+        for place, part in enumerate((zero, big, zero, small)):
+            qhi_ref[hw * place : hw * (place + 1), :] = part
         m_ref[...] = jnp.full(m_ref.shape, -1e30, f32)
         acc_ref[...] = jnp.zeros(acc_ref.shape, f32)
 
@@ -97,6 +101,7 @@
         c, t = units[u]
         at = pl.ds(tile * t, tile)
         k_pack = kv_ref[n * c : n * c + half, :]
+        k_pack = jnp.concatenate([k_pack, k_pack], axis=1)
         s_ref[u % 2, :half, :] = dot(k_pack, qlo_ref[:, at])
         s_ref[u % 2, half:, :] = dot(k_pack, qhi_ref[:, at])
 
@@ -104,10 +109,10 @@
         at = pl.ds(tile * units[u][1], tile)
         s = s_ref[u % 2]
         old = m_ref[:, at]
-        new = jnp.maximum(old, jnp.max(s, axis=0, keepdims=True) * LOG2E)
+        new = jnp.maximum(old, jnp.max(s, axis=0, keepdims=True))
         m_ref[:, at] = new
         shrink[u] = jnp.exp2(old - new)
-        p_ref[u % 2] = jnp.exp2(s * LOG2E - new).astype(bf16)
+        p_ref[u % 2] = jnp.exp2(s - new).astype(bf16)
 
     def values(u):
         c, t = units[u]
@@ -141,9 +146,10 @@
     x = at_ref[1]
     count = out_ref.shape[0]
     width = out_ref.shape[1] // count
+    base = w0.shape[0] - out_ref.shape[1]
     for j, w_ref in enumerate((w0, w1, w2, w3)):
         for d in range(count):
-            row = pl.multiple_of((x ^ d) * width, width)
+            row = pl.multiple_of(base + (x ^ d) * width, width)
             out_ref[j, width * d : width * (d + 1), :] = w_ref[pl.ds(row, width), :]
 
 
@@ -197,6 +203,20 @@
     out_ref[...] = dot(pick, normed).astype(bf16)
 
 
+def pack_body(at_ref, gate_ref, up_ref, mixer_ref, *out_refs):
+    y = at_ref[0]
+    count = len(out_refs)
+    hid, width = gate_ref.shape[0], out_refs[0].shape[1]
+    deep, rows = gate_ref.shape[1] // count, mixer_ref.shape[0] // count
+    for d, out_ref in enumerate(out_refs):
+        row = lax.rem(y + count - d, count)
+        for b in range(deep // width):
+            at = pl.ds(pl.multiple_of(row * deep + b * width, width), width)
+            out_ref[2 * hid * b : 2 * hid * b + hid, :] = gate_ref[:, at]
+            out_ref[2 * hid * b + hid : 2 * hid * (b + 1), :] = up_ref[:, at]
+        out_ref[2 * hid * deep // width :, :] = mixer_ref[pl.ds(pl.multiple_of(row * rows, rows), rows), :]
+
+
 def spread_body(x_ref, *refs):
     out_ref = refs[-1]
     cores, copies = 2, out_ref.shape[0] // 2
@@ -209,26 +229,25 @@
             out_ref[copies * c + i] = part
 
 
-def gate_up_body(at_ref, x_ref, w0_ref, w1_ref, w2_ref, w3_ref, *refs):
-    out_ref = refs[-1]
-    _, rows, width = x_ref.shape
+def gate_up_body(at_ref, x_ref, w0_ref, w1_ref, w2_ref, w3_ref, out_ref):
+    _, rows, _ = x_ref.shape
     y = at_ref[0]
     ws = (w0_ref, w1_ref, w2_ref, w3_ref)
-    blocks = w0_ref.shape[1] // width
+    hid = out_ref.shape[2]
+    blocks = x_ref.shape[0] // 2
     for j in range(0, len(ws), 2):
-        for c in range(x_ref.shape[0] // blocks):
+        for c in range(2):
             acc = None
             for b in range(blocks):
-                cols = slice(width * b, width * (b + 1))
-                w = jnp.concatenate([ws[j][:, cols], ws[j + 1][:, cols]], axis=0)
+                at = slice(hid * b, hid * (b + 1))
+                w = jnp.concatenate([ws[j][at, :], ws[j + 1][at, :]], axis=0)
                 term = lax.dot_general(
                     x_ref[blocks * c + b], w, (((1,), (1,)), ((), ())), preferred_element_type=f32
                 )
                 acc = term if acc is None else acc + term
-            half = acc.shape[1] // 2
             at = slice(rows * c, rows * (c + 1))
-            out_ref[y ^ j, at, :] = acc[:, :half].astype(bf16)
-            out_ref[y ^ (j + 1), at, :] = acc[:, half:].astype(bf16)
+            out_ref[lax.rem(y + j, len(ws)), at, :] = acc[:, :hid].astype(bf16)
+            out_ref[lax.rem(y + j + 1, len(ws)), at, :] = acc[:, hid:].astype(bf16)
 
 
 def hidden_body(parts_ref, out_ref):
@@ -248,7 +267,7 @@
 
 def down_body(h_ref, w_ref, after_ref, out_ref, wlo_ref, whi_ref):
     del after_ref
-    count, rows, width = h_ref.shape
+    count, _, width = h_ref.shape
     hid = width // 2
     zero = jnp.zeros((hid, w_ref.shape[1]), bf16)
     for j in range(count):
@@ -391,14 +410,17 @@
         compiler_params=params(),
         name="queries",
     )(query_input, query_gain[None, :], cos, sin)
-    both = jnp.concatenate([expert_gate[0].T, expert_up[0].T], axis=0)
-    deep = model // ny
-    gate_up = []
-    for d in range(ny):
-        part = lax.dynamic_slice_in_dim(both, (at_y ^ d) * deep, deep, 1)
-        if d:
-            part = lax.ppermute(part, "y", [(i, i ^ d) for i in range(ny)])
-        gate_up.append(part)
+    rows_y = mixer_out.shape[0] // ny
+    packs = pl.pallas_call(
+        pack_body,
+        out_shape=[jax.ShapeDtypeStruct((2 * hid * nx + rows_y, width), bf16)] * ny,
+        in_specs=[smem] + [vmem] * 3,
+        compiler_params=params(),
+        name="pack",
+    )(at_yx, expert_gate[0].T, expert_up[0].T, mixer_out)
+    moved = [packs[0]]
+    for d in range(1, ny):
+        moved.append(lax.ppermute(packs[d], "y", [(i, (i - d) % ny) for i in range(ny)]))
     pick, share = pl.pallas_call(
         lambda *refs: routing_body(*refs, experts=experts, cap=cap),
         out_shape=(
@@ -412,26 +434,18 @@
     block = pl.pallas_call(
         spread_body,
         out_shape=jax.ShapeDtypeStruct((2 * nx, slots // 2, width), bf16),
-        in_specs=[vmem] + [anywhere] * 5,
+        in_specs=[vmem] + [anywhere] * 3,
         compiler_params=params(),
         name="spread",
-    )(received, *gate_up[1:], q_t, pick)
+    )(received, q_t, pick, packs[0][:8, :128])
     block = lax.all_to_all(block, ("core", "x"), split_axis=0, concat_axis=0, tiled=True)
-    rows_y = mixer_out.shape[0] // ny
-    mixer = []
-    for d in range(ny):
-        part = lax.dynamic_slice_in_dim(mixer_out, (at_y ^ d) * rows_y, rows_y, 0)
-        if d:
-            part = lax.ppermute(part, "y", [(i, i ^ d) for i in range(ny)])
-        mixer.append(part)
-
     partial = pl.pallas_call(
         gate_up_body,
         out_shape=jax.ShapeDtypeStruct((ny, slots, 2 * hid), bf16),
-        in_specs=[smem] + [vmem] * 5 + [anywhere],
+        in_specs=[smem] + [vmem] * 5,
         compiler_params=params(),
         name="gate_up",
-    )(at_yx, block, *gate_up, sum(part[:8, :128] for part in mixer[1:]))
+    )(at_yx, block, *moved)
     partial = lax.all_to_all(partial, "y", split_axis=0, concat_axis=0, tiled=True)
     hidden = pl.pallas_call(
         hidden_body,
@@ -441,7 +455,7 @@
     )(partial)
     all_hidden = lax.all_to_all(hidden, TP, split_axis=0, concat_axis=0, tiled=True)
 
-    step_rows = 4 * seq
+    step_rows = 8 * seq
     attended = pl.pallas_call(
         lambda *refs: attend_body(*refs, n=seq, hw=hw, tile=256),
         out_shape=jax.ShapeDtypeStruct((seq, q_cols), bf16),
@@ -452,8 +466,8 @@
         ],
         out_specs=pl.BlockSpec((seq, q_cols), lambda i: (0, 0)),
         scratch_shapes=[
-            pltpu.VMEM((2 * hw, q_t.shape[1]), bf16),
-            pltpu.VMEM((2 * hw, q_t.shape[1]), bf16),
+            pltpu.VMEM((4 * hw, q_t.shape[1]), bf16),
+            pltpu.VMEM((4 * hw, q_t.shape[1]), bf16),
             pltpu.VMEM((1, q_t.shape[1]), f32),
             pltpu.VMEM((hw + 16, q_t.shape[1]), f32),
             pltpu.VMEM((2, seq, 256), f32),
@@ -491,7 +505,7 @@
         in_specs=[smem] + [vmem] * 4 + [anywhere],
         compiler_params=params(),
         name="weights",
-    )(at_yx, *mixer, attended[:8, :])
+    )(at_yx, *moved, attended[:8, :])
     mixed = pl.pallas_call(
         mixer_body,
         out_shape=[jax.ShapeDtypeStruct((seq, features), f32)]
@@ -501,7 +515,7 @@
     )(*parts, turned)
     sums = [mixed[0]]
     for d in range(1, ny):
-        sums.append(lax.ppermute(mixed[d], "y", [(i, i ^ d) for i in range(ny)]))
+        sums.append(lax.ppermute(mixed[d], "y", [(i, (i + d) % ny) for i in range(ny)]))
     attn_mixed = pl.pallas_call(
         mixed_body,
         out_shape=jax.ShapeDtypeStruct((seq, features), bf16),
@@ -535,6 +549,7 @@
         P(EP, None, TP),
         P(EP, None, TP),
     )
+
     return jax.shard_map(
         on_device,
         mesh=torus,

time: 194 us -> 200 us (1.031)
  waiting for transfers between devices: 36.7 us -> 45.5 us
  local copies, waits for them, and re-layouts: 8.31 us -> 13.6 us
  starting transfers between devices: 76.9 us -> 71.8 us
  Pallas kernels: 40.7 us -> 35.9 us
    all_to_all x1, waiting for transfers between devices: 0.01 us -> 14.2 us  [on_device(): lax.all_to_all(own.reshape(nz, 2 * cap, width), 'z', split_axis=0, concat...]
    ppermute x9 -> x6, starting transfers between devices: 29 us -> 19.9 us  [the longest x3 10.5 us: on_device(): lax.ppermute(mixed[d], 'y', [(i, (i + d) % ny) for i in range(ny)])]
    unnamed x38 -> x50, local copies, waits for them, and re-layouts: 6.34 us -> 13.6 us
    ppermute x9 -> x6, waiting for transfers between devices: 35 us -> 30.2 us  [the longest x3 23.1 us: on_device(): lax.ppermute(packs[d], 'y', [(i, (i - d) % ny) for i in range(ny)])]
    pallas_call x1, Pallas kernels: 24.3 us -> 19.5 us  [on_device(): pl.pallas_call(lambda *refs: attend_body(*refs, n=seq, hw=hw, tile=256),...]
    all_to_all x1, starting transfers between devices: 9.2 us -> 13.6 us  [on_device(): lax.all_to_all(block, ('core', 'x'), split_axis=0, concat_axis=0, tiled=T...]
  transfers between devices with their start and end apart: 17 -> 14, of which waited for: 9 -> 7; matrix products, arithmetic and copies ran while one was open for 1% -> 0% of each run, Pallas kernels for 18% -> 16%
where the time goes in v2:
time: 200 us; the launch traced here: 197 us
  starting transfers between devices  71.8 us (36%)
  waiting for transfers between devices  45.5 us (23%)
  Pallas kernels  35.9 us (18%)
  between operations  14.5 us (7%)
  blocking collectives  14.4 us (7%)
  local copies, waits for them, and re-layouts  13.6 us (7%)
    ppermute x3, waiting for transfers between devices, on_device(): lax.ppermute(packs[d], 'y', [(i, (i - d) % ny) for i in range(ny)])  23.1 us
    pallas_call x1, Pallas kernels, on_device(): pl.pallas_call(lambda *refs: attend_body(*refs, n=seq, hw=hw, tile=256),...  19.5 us
    all_to_all x1, starting transfers between devices, on_device(): lax.all_to_all(own.reshape(nz, 2 * cap, width), 'z', split_axis=0, concat...  15.9 us
    all_to_all x1, blocking collectives, on_device(): lax.all_to_all(partial, 'y', split_axis=0, concat_axis=0, tiled=True)  14.4 us
    all_to_all x1, waiting for transfers between devices, on_device(): lax.all_to_all(own.reshape(nz, 2 * cap, width), 'z', split_axis=0, concat...  14.2 us
    all_to_all x1, starting transfers between devices, on_device(): lax.all_to_all(block, ('core', 'x'), split_axis=0, concat_axis=0, tiled=T...  13.6 us
    unnamed x50, local copies, waits for them, and re-layouts  13.6 us
    ppermute x3, starting transfers between devices, on_device(): lax.ppermute(mixed[d], 'y', [(i, (i + d) % ny) for i in range(ny)])  10.5 us
  transfers between devices with their start and end apart: 14, of which 7 were waited for; matrix products, arithmetic and copies ran while one was open for 0% of the time, Pallas kernels for 16%

profile of v2, /device:TPU:1, one launch (start us, length us, event | category | flops | bytes accessed | tf_op | source)
XLA Modules:
  0.0 196.7 jit_solution(11325880171567730513)
XLA Ops:
  7.3 0.9 fusion
  8.2 2.6 %keys.1 = bf16[512,128]{1,0:T(8,128)(2,1)} custom-call(bf16[64,512]{1,0:T(8,128)(2,1)} %bitcast.30, bf16[64,512]{1,0:T(8,128)(2,1)} %bitcast.31, f32[1,64]{1,0:T(1,128)} %bitcast.33, f32[32,512]{1,0:T(8,128)} %get-tuple-element.23.cos_ref, f32[32,512]{1,0:T(8,128)} %get-tuple-element.22.sin_ref), custom_call_target="tpu_custom_call" | custom-call | tf_op jit(solution)/shard_map/keys/pallas_call | solution.py:374
  10.9 3.3 %dispatch.1 = bf16[768,256]{1,0:T(8,128)(2,1)} custom-call(s32[1]{0:T(128)} %bitcast.10.refs_0_, bf16[256,4096]{1,0:T(8,128)(2,1)} %refs_1_.1, f32[1,4096]{1,0:T(1,128)} %bitcast.32, s32[2,256]{1,0:T(2,128)} %bitcast.25), custom_call_target="tpu_custom_call" | custom-call | tf_op jit(solution)/shard_map/dispatch/pallas_call | solution.py:389
  14.3 15.9 %all-to-all-start = ((bf16[16,48,256]{2,1,0:T(8,128)(2,1)}), bf16[16,48,256]{2,1,0:T(8,128)(2,1)S(1)}, u32[]{:S(2)}, u32[]{:S(2)}) async-start(bf16[16,48,256]{2,1,0:T(8,128)(2,1)} %bitcast.29), calls=%async_computation | async-start | bytes 786432 | tf_op jit(solution)/shard_map/all_to_all | solution.py:403
  30.2 1.0 routing.1
  31.2 0.7 copy-done.15
  32.0 1.1 copy-done.11
  33.1 0.7 pack.1
  33.8 0.8 copy-done.22
  35.2 14.2 %all-to-all-done.x_ref = bf16[16,48,256]{2,1,0:T(8,128)(2,1)S(1)} async-done(((bf16[16,48,256]{2,1,0:T(8,128)(2,1)}), bf16[16,48,256]{2,1,0:T(8,128)(2,1)S(1)}, u32[]{:S(2)}, u32[]{:S(2)}) %all-to-all-start) | async-done | bytes 393248 | tf_op jit(solution)/shard_map/all_to_all | solution.py:403
  49.3 1.3 spread.1
  50.7 13.6 %all-to-all-start.1 = ((bf16[8,384,256]{2,1,0:T(8,128)(2,1)}), bf16[8,384,256]{2,1,0:T(8,128)(2,1)S(1)}, u32[]{:S(2)}, u32[]{:S(2)}) async-start(bf16[8,384,256]{2,1,0:T(8,128)(2,1)} %spread.1), calls=%async_computation.1 | async-start | bytes 3145728 | tf_op jit(solution)/shard_map/all_to_all | solution.py:441
  64.3 4.6 %collective-permute-start.3 = (bf16[1024,256]{1,0:T(8,128)(2,1)}, bf16[1024,256]{1,0:T(8,128)(2,1)S(1)}, u32[]{:S(2)}, u32[]{:S(2)}) collective-permute-start(bf16[1024,256]{1,0:T(8,128)(2,1)} %copy-done.24), channel_id=1, source_target_pairs={{0,12},{4,0},{8,4},{12,8},{1,13},{5,1},{9,5},{13,9},{2,14},{6,2},{... | collective-permute-start | bytes 1572872 | tf_op jit(solution)/shard_map/ppermute | solution.py:423
  68.9 2.2 %collective-permute-start.4 = (bf16[1024,256]{1,0:T(8,128)(2,1)}, bf16[1024,256]{1,0:T(8,128)(2,1)S(1)}, u32[]{:S(2)}, u32[]{:S(2)}) collective-permute-start(bf16[1024,256]{1,0:T(8,128)(2,1)} %copy-done.23), channel_id=1, source_target_pairs={{0,8},{4,12},{8,0},{12,4},{1,9},{5,13},{9,1},{13,5},{2,10},{6,14},... | collective-permute-start | bytes 1572872 | tf_op jit(solution)/shard_map/ppermute | solution.py:423
  71.2 2.6 %collective-permute-start.5 = (bf16[1024,256]{1,0:T(8,128)(2,1)}, bf16[1024,256]{1,0:T(8,128)(2,1)S(1)}, u32[]{:S(2)}, u32[]{:S(2)}) collective-permute-start(bf16[1024,256]{1,0:T(8,128)(2,1)} %copy-done.22), channel_id=1, source_target_pairs={{0,4},{4,8},{8,12},{12,0},{1,5},{5,9},{9,13},{13,1},{2,6},{6,10},{... | collective-permute-start | bytes 1572872 | tf_op jit(solution)/shard_map/ppermute | solution.py:423
  73.8 17.8 %collective-permute-done.3.w1.w1_ref = bf16[1024,256]{1,0:T(8,128)(2,1)S(1)} collective-permute-done((bf16[1024,256]{1,0:T(8,128)(2,1)}, bf16[1024,256]{1,0:T(8,128)(2,1)S(1)}, u32[]{:S(2)}, u32[]{:S(2)}) %collective-permute-start.3) | collective-permute-done | bytes 524320 | tf_op jit(solution)/shard_map/ppermute | solution.py:423
  91.6 0.8 copy-done
  92.4 5.3 %collective-permute-done.5.w3.w3_ref = bf16[1024,256]{1,0:T(8,128)(2,1)S(1)} collective-permute-done((bf16[1024,256]{1,0:T(8,128)(2,1)}, bf16[1024,256]{1,0:T(8,128)(2,1)S(1)}, u32[]{:S(2)}, u32[]{:S(2)}) %collective-permute-start.5) | collective-permute-done | bytes 524320 | tf_op jit(solution)/shard_map/ppermute | solution.py:423
  97.7 0.8 copy-done.3
  98.5 1.0 copy-done.1
  99.5 1.0 copy-done.4
  100.6 1.5 gate_up.1
  102.1 14.4 %all_to_all.25.parts_ref = bf16[4,768,128]{2,1,0:T(8,128)(2,1)S(1)} all-to-all(bf16[4,768,128]{2,1,0:T(8,128)(2,1)S(1)} %gate_up.1), channel_id=1, replica_groups=mesh['z'=16,'core'=2,'y'=4,'x'=4] {'y'}, dimensions={0} | all-to-all | bytes 1572864 | tf_op jit(solution)/shard_map/all_to_all | solution.py:449
  116.5 1.6 hidden.1
  118.0 4.7 %all-to-all-start.3 = ((bf16[16,384,128]{2,1,0:T(8,128)(2,1)}), bf16[16,384,128]{2,1,0:T(8,128)(2,1)S(1)}, u32[]{:S(2)}, u32[]{:S(2)}) async-start(bf16[16,384,128]{2,1,0:T(8,128)(2,1)} %hidden.1), calls=%async_computation.3 | async-start | bytes 3145728 | tf_op jit(solution)/shard_map/all_to_all | solution.py:456
  122.8 0.9 copy-done.14
  123.7 2.2 %copy-done.21 = bf16[16384,128]{1,0:T(8,128)(2,1)S(1)} copy-done((bf16[16384,128]{1,0:T(8,128)(2,1)S(1)}, bf16[16384,128]{1,0:T(8,128)(2,1)}, u32[]{:S(2)}) %copy-start.21) | copy-done | bytes 4194328
  125.9 19.5 %attend.1.a0.after_ref = bf16[512,128]{1,0:T(8,128)(2,1)S(1)} custom-call(bf16[64,1024]{1,0:T(8,128)(2,1)S(1)} %copy-done.14, bf16[16384,128]{1,0:T(8,128)(2,1)S(1)} %copy-done.21), custom_call_target="tpu_custom_call" | custom-call | flops 4294967296 | bytes 4194304 | tf_op jit(solution)/shard_map/attend/pallas_call | solution.py:459
  145.4 1.0 copy-done.12
  146.5 1.0 down.1
  147.5 0.7 copy-done.6
  148.2 8.6 %all-to-all-start.4 = ((bf16[32,24,256]{2,1,0:T(8,128)(2,1)}), bf16[32,24,256]{2,1,0:T(8,128)(2,1)S(1)}, u32[]{:S(2)}, u32[]{:S(2)}) async-start(bf16[32,24,256]{2,1,0:T(8,128)(2,1)} %bitcast.20), calls=%async_computation.4 | async-start | bytes 786432 | tf_op jit(solution)/shard_map/all_to_all | solution.py:497
  156.8 4.2 %collective-permute-start.2 = (bf16[512,128]{1,0:T(8,128)(2,1)S(1)}, bf16[512,128]{1,0:T(8,128)(2,1)S(1)}, u32[]{:S(2)}, u32[]{:S(2)}) collective-permute-start(bf16[512,128]{1,0:T(8,128)(2,1)S(1)} %attend.1.a0.after_ref), channel_id=1, source_target_pairs={{0,3},{1,2},{2,1},{3,0},{4,7},{5,6},{6,5},{7,4},{8,11},{9,10},{10,... | collective-permute-start | bytes 393224 | tf_op jit(solution)/shard_map/ppermute | solution.py:484
  161.0 2.5 %collective-permute-start.1 = (bf16[512,128]{1,0:T(8,128)(2,1)S(1)}, bf16[512,128]{1,0:T(8,128)(2,1)S(1)}, u32[]{:S(2)}, u32[]{:S(2)}) collective-permute-start(bf16[512,128]{1,0:T(8,128)(2,1)S(1)} %attend.1.a0.after_ref), channel_id=1, source_target_pairs={{0,2},{1,3},{2,0},{3,1},{4,6},{5,7},{6,4},{7,5},{8,10},{9,11},{10,... | collective-permute-start | bytes 393224 | tf_op jit(solution)/shard_map/ppermute | solution.py:484
  163.5 2.3 %collective-permute-start = (bf16[512,128]{1,0:T(8,128)(2,1)S(1)}, bf16[512,128]{1,0:T(8,128)(2,1)S(1)}, u32[]{:S(2)}, u32[]{:S(2)}) collective-permute-start(bf16[512,128]{1,0:T(8,128)(2,1)S(1)} %attend.1.a0.after_ref), channel_id=1, source_target_pairs={{0,1},{1,0},{2,3},{3,2},{4,5},{5,4},{6,7},{7,6},{8,9},{9,8},{10,11... | collective-permute-start | bytes 393224 | tf_op jit(solution)/shard_map/ppermute | solution.py:484
  165.8 1.0 copy-done.2
  166.9 1.0 copy-done.5
  167.9 0.6 weights.1.w_ref
  168.5 0.4 collective-permute-done.1.a2
  169.0 0.7 collective-permute-done.a1
  169.7 0.7 mixer.1
  170.4 3.1 %collective-permute-start.6 = (bf16[512,256]{1,0:T(8,128)(2,1)S(1)}, bf16[512,256]{1,0:T(8,128)(2,1)S(1)}, u32[]{:S(2)}, u32[]{:S(2)}) collective-permute-start(bf16[512,256]{1,0:T(8,128)(2,1)S(1)} %get-tuple-element.17), channel_id=1, source_target_pairs={{0,4},{4,8},{8,12},{12,0},{1,5},{5,9},{9,13},{13,1},{2,6},{6,10},{... | collective-permute-start | bytes 786440 | tf_op jit(solution)/shard_map/ppermute | solution.py:518
  173.5 4.3 %collective-permute-start.7 = (bf16[512,256]{1,0:T(8,128)(2,1)S(1)}, bf16[512,256]{1,0:T(8,128)(2,1)S(1)}, u32[]{:S(2)}, u32[]{:S(2)}) collective-permute-start(bf16[512,256]{1,0:T(8,128)(2,1)S(1)} %get-tuple-element.18), channel_id=1, source_target_pairs={{0,8},{4,12},{8,0},{12,4},{1,9},{5,13},{9,1},{13,5},{2,10},{6,14},... | collective-permute-start | bytes 786440 | tf_op jit(solution)/shard_map/ppermute | solution.py:518
  177.8 3.1 %collective-permute-start.8 = (bf16[512,256]{1,0:T(8,128)(2,1)S(1)}, bf16[512,256]{1,0:T(8,128)(2,1)S(1)}, u32[]{:S(2)}, u32[]{:S(2)}) collective-permute-start(bf16[512,256]{1,0:T(8,128)(2,1)S(1)} %get-tuple-element.19), channel_id=1, source_target_pairs={{0,12},{4,0},{8,4},{12,8},{1,13},{5,1},{9,5},{13,9},{2,14},{6,2},{... | collective-permute-start | bytes 786440 | tf_op jit(solution)/shard_map/ppermute | solution.py:518
  180.9 5.3 %collective-permute-done.7.r2_ref = bf16[512,256]{1,0:T(8,128)(2,1)S(1)} collective-permute-done((bf16[512,256]{1,0:T(8,128)(2,1)S(1)}, bf16[512,256]{1,0:T(8,128)(2,1)S(1)}, u32[]{:S(2)}, u32[]{:S(2)}) %collective-permute-start.7) | collective-permute-done | bytes 262176 | tf_op jit(solution)/shard_map/ppermute | solution.py:518
  186.2 1.8 collective-permute-done.8.r3_ref
  188.0 0.8 mixed.1
  188.9 1.0 combine.1
  (53 shorter events, 0.9 us)
Async XLA Ops:
  7.2 115.6 %all-gather.2.cloned.1.call-start = ((), (), s32[]{:S(2)}) async-start(), calls=%async_computation.5 | async-start | bytes 4325376 | tf_op jit(solution)/shard_map/all_gather | solution.py:387
  10.9 19.3 %copy-start.18 = (s32[256,2]{0,1:T(2,128)S(1)}, s32[256,2]{0,1:T(2,128)}, u32[]{:S(2)}) copy-start(s32[256,2]{0,1:T(2,128)} %param.21) | copy-start | bytes 6148
  10.9 19.3 %copy-start.19 = (f32[256,2]{0,1:T(2,128)S(1)}, f32[256,2]{0,1:T(2,128)}, u32[]{:S(2)}) copy-start(f32[256,2]{0,1:T(2,128)} %param.22) | copy-start | bytes 6148
  10.9 21.1 %copy-start.7 = (bf16[2048,256]{1,0:T(8,128)(2,1)S(1)}, bf16[2048,256]{1,0:T(8,128)(2,1)}, u32[]{:S(2)}) copy-start(bf16[2048,256]{1,0:T(8,128)(2,1)} %mixer_ref.1) | copy-start | bytes 3145732
  10.9 21.1 %copy-start.10 = (bf16[1,4096,64]{1,2,0:T(8,128)(2,1)S(1)}, bf16[1,4096,64]{1,2,0:T(8,128)(2,1)}, u32[]{:S(2)}) copy-start(bf16[1,4096,64]{1,2,0:T(8,128)(2,1)} %param.23) | copy-start | bytes 1572868
  14.2 20.7 %copy-start.8 = (f32[32,512]{1,0:T(8,128)S(1)}, f32[32,512]{1,0:T(8,128)}, u32[]{:S(2)}) copy-start(f32[32,512]{1,0:T(8,128)} %get-tuple-element.22.sin_ref) | copy-start | bytes 196612
  14.3 20.7 %copy-start.9 = (f32[32,512]{1,0:T(8,128)S(1)}, f32[32,512]{1,0:T(8,128)}, u32[]{:S(2)}) copy-start(f32[32,512]{1,0:T(8,128)} %get-tuple-element.23.cos_ref) | copy-start | bytes 196612
  14.3 20.7 %copy-start.17 = (bf16[512,128]{1,0:T(8,128)(2,1)S(1)}, bf16[512,128]{1,0:T(8,128)(2,1)}, u32[]{:S(2)}) copy-start(bf16[512,128]{1,0:T(8,128)(2,1)} %q_ref.1) | copy-start | bytes 393220
  14.3 20.7 %copy-start.20 = (f32[64]{0:T(128)S(1)}, f32[64]{0:T(128)}, u32[]{:S(2)}) copy-start(f32[64]{0:T(128)} %param.16) | copy-start | bytes 772
  14.3 35.0 %all-to-all-start = ((bf16[16,48,256]{2,1,0:T(8,128)(2,1)}), bf16[16,48,256]{2,1,0:T(8,128)(2,1)S(1)}, u32[]{:S(2)}, u32[]{:S(2)}) async-start(bf16[16,48,256]{2,1,0:T(8,128)(2,1)} %bitcast.29), calls=%async_computation | async-start | bytes 786432 | tf_op jit(solution)/shard_map/all_to_all | solution.py:403
  31.2 0.7 copy-start.15
  32.0 1.1 copy-start.11
  33.8 0.8 copy-start.22
  33.8 1.0 copy-start.23
  33.8 1.1 copy-start.24
  35.2 15.5 %copy-start.13 = (bf16[64,1024]{1,0:T(8,128)(2,1)}, bf16[64,1024]{1,0:T(8,128)(2,1)S(1)}, u32[]{:S(2)}) copy-start(bf16[64,1024]{1,0:T(8,128)(2,1)S(1)} %queries.1.refs_0_) | copy-start | bytes 393220
  50.7 47.8 %all-to-all-start.1 = ((bf16[8,384,256]{2,1,0:T(8,128)(2,1)}), bf16[8,384,256]{2,1,0:T(8,128)(2,1)S(1)}, u32[]{:S(2)}, u32[]{:S(2)}) async-start(bf16[8,384,256]{2,1,0:T(8,128)(2,1)} %spread.1), calls=%async_computation.1 | async-start | bytes 3145728 | tf_op jit(solution)/shard_map/all_to_all | solution.py:441
  64.3 27.3 %collective-permute-start.3 = (bf16[1024,256]{1,0:T(8,128)(2,1)}, bf16[1024,256]{1,0:T(8,128)(2,1)S(1)}, u32[]{:S(2)}, u32[]{:S(2)}) collective-permute-start(bf16[1024,256]{1,0:T(8,128)(2,1)} %copy-done.24), channel_id=1, source_target_pairs={{0,12},{4,0},{8,4},{12,8},{1,13},{5,1},{9,5},{13,9},{2,14},{6,2},{... | collective-permute-start | bytes 1572872 | tf_op jit(solution)/shard_map/ppermute | solution.py:423
  68.9 22.7 %collective-permute-start.4 = (bf16[1024,256]{1,0:T(8,128)(2,1)}, bf16[1024,256]{1,0:T(8,128)(2,1)S(1)}, u32[]{:S(2)}, u32[]{:S(2)}) collective-permute-start(bf16[1024,256]{1,0:T(8,128)(2,1)} %copy-done.23), channel_id=1, source_target_pairs={{0,8},{4,12},{8,0},{12,4},{1,9},{5,13},{9,1},{13,5},{2,10},{6,14},... | collective-permute-start | bytes 1572872 | tf_op jit(solution)/shard_map/ppermute | solution.py:423
  71.2 26.5 %collective-permute-start.5 = (bf16[1024,256]{1,0:T(8,128)(2,1)}, bf16[1024,256]{1,0:T(8,128)(2,1)S(1)}, u32[]{:S(2)}, u32[]{:S(2)}) collective-permute-start(bf16[1024,256]{1,0:T(8,128)(2,1)} %copy-done.22), channel_id=1, source_target_pairs={{0,4},{4,8},{8,12},{12,0},{1,5},{5,9},{9,13},{13,1},{2,6},{6,10},{... | collective-permute-start | bytes 1572872 | tf_op jit(solution)/shard_map/ppermute | solution.py:423
  91.6 0.8 copy-start
  97.7 0.8 copy-start.3
  98.5 1.0 copy-start.1
  99.5 1.0 copy-start.4
  118.0 27.4 %all-to-all-start.3 = ((bf16[16,384,128]{2,1,0:T(8,128)(2,1)}), bf16[16,384,128]{2,1,0:T(8,128)(2,1)S(1)}, u32[]{:S(2)}, u32[]{:S(2)}) async-start(bf16[16,384,128]{2,1,0:T(8,128)(2,1)} %hidden.1), calls=%async_computation.3 | async-start | bytes 3145728 | tf_op jit(solution)/shard_map/all_to_all | solution.py:456
  122.8 0.9 copy-start.14
  123.7 2.2 %copy-start.21 = (bf16[16384,128]{1,0:T(8,128)(2,1)S(1)}, bf16[16384,128]{1,0:T(8,128)(2,1)}, u32[]{:S(2)}) copy-start(bf16[16384,128]{1,0:T(8,128)(2,1)} %all-gather.2.cloned.1.call-done.refs_1_) | copy-start | bytes 12582916
  145.4 1.0 copy-start.12
  147.5 0.7 copy-start.6
  148.2 40.7 %all-to-all-start.4 = ((bf16[32,24,256]{2,1,0:T(8,128)(2,1)}), bf16[32,24,256]{2,1,0:T(8,128)(2,1)S(1)}, u32[]{:S(2)}, u32[]{:S(2)}) async-start(bf16[32,24,256]{2,1,0:T(8,128)(2,1)} %bitcast.20), calls=%async_computation.4 | async-start | bytes 786432 | tf_op jit(solution)/shard_map/all_to_all | solution.py:497
  156.8 11.7 %collective-permute-start.2 = (bf16[512,128]{1,0:T(8,128)(2,1)S(1)}, bf16[512,128]{1,0:T(8,128)(2,1)S(1)}, u32[]{:S(2)}, u32[]{:S(2)}) collective-permute-start(bf16[512,128]{1,0:T(8,128)(2,1)S(1)} %attend.1.a0.after_ref), channel_id=1, source_target_pairs={{0,3},{1,2},{2,1},{3,0},{4,7},{5,6},{6,5},{7,4},{8,11},{9,10},{10,... | collective-permute-start | bytes 393224 | tf_op jit(solution)/shard_map/ppermute | solution.py:484
  161.0 7.9 %collective-permute-start.1 = (bf16[512,128]{1,0:T(8,128)(2,1)S(1)}, bf16[512,128]{1,0:T(8,128)(2,1)S(1)}, u32[]{:S(2)}, u32[]{:S(2)}) collective-permute-start(bf16[512,128]{1,0:T(8,128)(2,1)S(1)} %attend.1.a0.after_ref), channel_id=1, source_target_pairs={{0,2},{1,3},{2,0},{3,1},{4,6},{5,7},{6,4},{7,5},{8,10},{9,11},{10,... | collective-permute-start | bytes 393224 | tf_op jit(solution)/shard_map/ppermute | solution.py:484
  163.5 6.1 %collective-permute-start = (bf16[512,128]{1,0:T(8,128)(2,1)S(1)}, bf16[512,128]{1,0:T(8,128)(2,1)S(1)}, u32[]{:S(2)}, u32[]{:S(2)}) collective-permute-start(bf16[512,128]{1,0:T(8,128)(2,1)S(1)} %attend.1.a0.after_ref), channel_id=1, source_target_pairs={{0,1},{1,0},{2,3},{3,2},{4,5},{5,4},{6,7},{7,6},{8,9},{9,8},{10,11... | collective-permute-start | bytes 393224 | tf_op jit(solution)/shard_map/ppermute | solution.py:484
  165.8 1.0 copy-start.2
  166.9 1.0 copy-start.5
  168.5 20.3 %copy-start.16 = (f32[2,256,128]{2,1,0:T(8,128)S(1)}, f32[2,256,128]{2,1,0:T(8,128)}, u32[]{:S(2)}) copy-start(f32[2,256,128]{2,1,0:T(8,128)} %copy-done.15) | copy-start | bytes 786436
  170.4 10.5 %collective-permute-start.6 = (bf16[512,256]{1,0:T(8,128)(2,1)S(1)}, bf16[512,256]{1,0:T(8,128)(2,1)S(1)}, u32[]{:S(2)}, u32[]{:S(2)}) collective-permute-start(bf16[512,256]{1,0:T(8,128)(2,1)S(1)} %get-tuple-element.17), channel_id=1, source_target_pairs={{0,4},{4,8},{8,12},{12,0},{1,5},{5,9},{9,13},{13,1},{2,6},{6,10},{... | collective-permute-start | bytes 786440 | tf_op jit(solution)/shard_map/ppermute | solution.py:518
  173.5 12.7 %collective-permute-start.7 = (bf16[512,256]{1,0:T(8,128)(2,1)S(1)}, bf16[512,256]{1,0:T(8,128)(2,1)S(1)}, u32[]{:S(2)}, u32[]{:S(2)}) collective-permute-start(bf16[512,256]{1,0:T(8,128)(2,1)S(1)} %get-tuple-element.18), channel_id=1, source_target_pairs={{0,8},{4,12},{8,0},{12,4},{1,9},{5,13},{9,1},{13,5},{2,10},{6,14},... | collective-permute-start | bytes 786440 | tf_op jit(solution)/shard_map/ppermute | solution.py:518
  177.8 10.2 %collective-permute-start.8 = (bf16[512,256]{1,0:T(8,128)(2,1)S(1)}, bf16[512,256]{1,0:T(8,128)(2,1)S(1)}, u32[]{:S(2)}, u32[]{:S(2)}) collective-permute-start(bf16[512,256]{1,0:T(8,128)(2,1)S(1)} %get-tuple-element.19), channel_id=1, source_target_pairs={{0,12},{4,0},{8,4},{12,8},{1,13},{5,1},{9,5},{13,9},{2,14},{6,2},{... | collective-permute-start | bytes 786440 | tf_op jit(solution)/shard_map/ppermute | solution.py:518
Sparse Core Ops, SparseCore 0:
  11.0 88.5 all-gather.1

commit v3 on v2

--- a/solution.py
+++ b/solution.py
@@ -48,11 +48,7 @@
     return jnp.sum(jnp.where(same, row, 0.0), axis=1, keepdims=True)
 
 
-def key_body(
-    k_hbm, v_hbm, gain_hbm, cos_ref, sin_ref, chunk_ref, k_ref, v_ref, gain_ref, sems
-):
-    for copy in start_copies(((k_hbm, k_ref), (v_hbm, v_ref), (gain_hbm, gain_ref)), sems):
-        copy.wait()
+def key_chunk(k_ref, v_ref, gain_ref, cos_ref, sin_ref, chunk_ref):
     hw, n = k_ref.shape
     k_t = norm_turn(k_ref[...].astype(f32), column(gain_ref[...]), cos_ref[...], sin_ref[...])
     k_t = k_t.astype(bf16).astype(f32)
@@ -169,13 +165,15 @@
     out_ref[...] = total.astype(bf16)
 
 
-def dispatch_body(
-    at_ref, x_hbm, gain_hbm, routes_hbm, out_ref, x_ref, gain_ref, routes_ref, sems, *, experts, cap
-):
-    pairs = ((routes_hbm, routes_ref), (x_hbm, x_ref), (gain_hbm, gain_ref))
-    copies = start_copies(pairs, sems)
+def front_body(at_ref, *refs, experts, cap):
+    inputs, (chunk_ref, out_ref), held, sems = refs[:8], refs[8:10], refs[10:18], refs[18]
+    copies = start_copies(tuple(zip(inputs, held)), sems)
+    x_ref, gain_ref, routes_ref = held[5:]
+    for copy in copies[:5]:
+        copy.wait()
+    key_chunk(*held[:5], chunk_ref)
     rows = x_ref.shape[0]
-    copies[0].wait()
+    copies[7].wait()
     ids = lax.broadcasted_iota(jnp.int32, (experts, rows), 0)
     hits = jnp.zeros((experts, rows), f32)
     for k in range(routes_ref.shape[0]):
@@ -193,8 +191,8 @@
     place = lax.broadcasted_iota(jnp.int32, (slots, rows), 0)
     want = (lax.rem(place, jnp.full_like(place, cap)) + 1).astype(f32)
     pick = (wide == want).astype(f32).astype(bf16)
-    copies[1].wait()
-    copies[2].wait()
+    copies[5].wait()
+    copies[6].wait()
     x = x_ref[...].astype(f32)
     width = out_ref.shape[1]
     own = pl.ds(pl.multiple_of(at_ref[0] * width, width), width)
@@ -371,34 +369,30 @@
         [inverse[:, None] * row[None, :], inverse[:, None] * col[None, :]], axis=0
     )
     cos, sin = jnp.cos(angles), jnp.sin(angles)
-    chunk = pl.pallas_call(
-        key_body,
-        out_shape=jax.ShapeDtypeStruct((seq, 2 * hw), bf16),
-        in_specs=[hbm, hbm, hbm, vmem, vmem],
-        scratch_shapes=[
-            pltpu.VMEM((hw, seq), bf16),
-            pltpu.VMEM((hw, seq), bf16),
-            pltpu.VMEM((1, hw), f32),
-            pltpu.SemaphoreType.DMA((3,)),
-        ],
+    held = (
+        key_input.T,
+        value_input.T,
+        key_gain[None, :],
+        cos,
+        sin,
+        moe_input,
+        moe_gain[None, :],
+        routes.T,
+    )
+    chunk, own = pl.pallas_call(
+        lambda *refs: front_body(*refs, experts=experts, cap=cap),
+        out_shape=(
+            jax.ShapeDtypeStruct((seq, 2 * hw), bf16),
+            jax.ShapeDtypeStruct((slots, width), bf16),
+        ),
+        in_specs=[smem] + [hbm] * len(held),
+        scratch_shapes=[pltpu.VMEM(a.shape, a.dtype) for a in held]
+        + [pltpu.SemaphoreType.DMA((len(held),))],
         compiler_params=params(60),
-        name="keys",
-    )(key_input.T, value_input.T, key_gain[None, :], cos, sin)
+        name="front",
+    )(lax.axis_index(TP)[None].astype(jnp.int32), *held)
     keys = lax.all_gather(chunk, EP, axis=0, tiled=True)
 
-    own = pl.pallas_call(
-        lambda *refs: dispatch_body(*refs, experts=experts, cap=cap),
-        out_shape=jax.ShapeDtypeStruct((slots, width), bf16),
-        in_specs=[smem, hbm, hbm, hbm],
-        scratch_shapes=[
-            pltpu.VMEM((tokens, model), bf16),
-            pltpu.VMEM((1, model), f32),
-            pltpu.VMEM((routes.shape[1], tokens), jnp.int32),
-            pltpu.SemaphoreType.DMA((3,)),
-        ],
-        compiler_params=params(60),
-        name="dispatch",
-    )(lax.axis_index(TP)[None].astype(jnp.int32), moe_input, moe_gain[None, :], routes.T)
     nz = lax.axis_size("z")
     received = lax.all_to_all(
         own.reshape(nz, 2 * cap, width), "z", split_axis=0, concat_axis=0, tiled=True
@@ -455,7 +449,7 @@
     )(partial)
     all_hidden = lax.all_to_all(hidden, TP, split_axis=0, concat_axis=0, tiled=True)
 
-    step_rows = 8 * seq
+    step_rows = 16 * seq
     attended = pl.pallas_call(
         lambda *refs: attend_body(*refs, n=seq, hw=hw, tile=256),
         out_shape=jax.ShapeDtypeStruct((seq, q_cols), bf16),

time: 200 us -> 196 us (0.980)
  Pallas kernels: 35.9 us -> 32.9 us
    pallas_call x2 -> x1, Pallas kernels: 5.93 us -> 3.68 us  [on_device(): pl.pallas_call(lambda *refs: front_body(*refs, experts=experts, cap=cap),...]
  transfers between devices with their start and end apart: 14 -> 14, of which waited for: 7 -> 7; matrix products, arithmetic and copies ran while one was open for 0% -> 0% of each run, Pallas kernels for 16% -> 14%
where the time goes in v3:
time: 196 us; the launch traced here: 194 us
  starting transfers between devices  70.9 us (36%)
  waiting for transfers between devices  47.2 us (24%)
  Pallas kernels  32.9 us (17%)
  between operations  14.4 us (7%)
  blocking collectives  14.3 us (7%)
  local copies, waits for them, and re-layouts  13.6 us (7%)
    ppermute x3, waiting for transfers between devices, on_device(): lax.ppermute(packs[d], 'y', [(i, (i - d) % ny) for i in range(ny)])  23.1 us
    pallas_call x1, Pallas kernels, on_device(): pl.pallas_call(lambda *refs: attend_body(*refs, n=seq, hw=hw, tile=256),...  18.8 us
    all_to_all x1, starting transfers between devices, on_device(): lax.all_to_all(own.reshape(nz, 2 * cap, width), 'z', split_axis=0, concat...  15.9 us
    all_to_all x1, blocking collectives, on_device(): lax.all_to_all(partial, 'y', split_axis=0, concat_axis=0, tiled=True)  14.3 us
    all_to_all x1, waiting for transfers between devices, on_device(): lax.all_to_all(own.reshape(nz, 2 * cap, width), 'z', split_axis=0, concat...  13.9 us
    unnamed x50, local copies, waits for them, and re-layouts  13.6 us
    all_to_all x1, starting transfers between devices, on_device(): lax.all_to_all(block, ('core', 'x'), split_axis=0, concat_axis=0, tiled=T...  13.6 us
    ppermute x3, starting transfers between devices, on_device(): lax.ppermute(packs[d], 'y', [(i, (i - d) % ny) for i in range(ny)])  9.57 us
  transfers between devices with their start and end apart: 14, of which 7 were waited for; matrix products, arithmetic and copies ran while one was open for 0% of the time, Pallas kernels for 14%

profile of v3, /device:TPU:1, one launch (start us, length us, event | category | flops | bytes accessed | tf_op | source)
XLA Modules:
  0.0 194.4 jit_solution(3360357454474851088)
XLA Ops:
  7.3 0.9 fusion
  8.2 3.7 %front.1 = (bf16[512,128]{1,0:T(8,128)(2,1)}, bf16[768,256]{1,0:T(8,128)(2,1)}) custom-call(s32[1]{0:T(128)} %bitcast.1.refs_0_, bf16[64,512]{1,0:T(8,128)(2,1)} %bitcast.30, bf16[64,512]{1,0:T(8,128)(2,1)} %bitcast.31, f32[1,64]{1,0:T(1,128)} %bitcast.33, f32[32,512]{1,0:T(8,128)} %get-tuple-element.27.cos_ref.refs_4_, ...), custom_call_target="tpu_custom_call" | custom-call | tf_op jit(solution)/shard_map/front/pallas_call | solution.py:382
  12.0 15.9 %all-to-all-start = ((bf16[16,48,256]{2,1,0:T(8,128)(2,1)}), bf16[16,48,256]{2,1,0:T(8,128)(2,1)S(1)}, u32[]{:S(2)}, u32[]{:S(2)}) async-start(bf16[16,48,256]{2,1,0:T(8,128)(2,1)} %bitcast.29), calls=%async_computation | async-start | bytes 786432 | tf_op jit(solution)/shard_map/all_to_all | solution.py:397
  27.9 1.0 routing.1
  28.9 0.7 copy-done.15
  29.7 1.0 copy-done.11
  30.7 0.7 pack.1
  31.5 0.8 copy-done.22
  32.6 0.2 queries.1.refs_0_
  32.9 13.9 %all-to-all-done.x_ref = bf16[16,48,256]{2,1,0:T(8,128)(2,1)S(1)} async-done(((bf16[16,48,256]{2,1,0:T(8,128)(2,1)}), bf16[16,48,256]{2,1,0:T(8,128)(2,1)S(1)}, u32[]{:S(2)}, u32[]{:S(2)}) %all-to-all-start) | async-done | bytes 393248 | tf_op jit(solution)/shard_map/all_to_all | solution.py:397
  46.8 1.3 spread.1
  48.1 13.6 %all-to-all-start.1 = ((bf16[8,384,256]{2,1,0:T(8,128)(2,1)}), bf16[8,384,256]{2,1,0:T(8,128)(2,1)S(1)}, u32[]{:S(2)}, u32[]{:S(2)}) async-start(bf16[8,384,256]{2,1,0:T(8,128)(2,1)} %spread.1), calls=%async_computation.1 | async-start | bytes 3145728 | tf_op jit(solution)/shard_map/all_to_all | solution.py:435
  61.6 4.7 %collective-permute-start.3 = (bf16[1024,256]{1,0:T(8,128)(2,1)}, bf16[1024,256]{1,0:T(8,128)(2,1)S(1)}, u32[]{:S(2)}, u32[]{:S(2)}) collective-permute-start(bf16[1024,256]{1,0:T(8,128)(2,1)} %copy-done.24), channel_id=1, source_target_pairs={{0,12},{4,0},{8,4},{12,8},{1,13},{5,1},{9,5},{13,9},{2,14},{6,2},{... | collective-permute-start | bytes 1572872 | tf_op jit(solution)/shard_map/ppermute | solution.py:417
  66.4 2.2 %collective-permute-start.4 = (bf16[1024,256]{1,0:T(8,128)(2,1)}, bf16[1024,256]{1,0:T(8,128)(2,1)S(1)}, u32[]{:S(2)}, u32[]{:S(2)}) collective-permute-start(bf16[1024,256]{1,0:T(8,128)(2,1)} %copy-done.23), channel_id=1, source_target_pairs={{0,8},{4,12},{8,0},{12,4},{1,9},{5,13},{9,1},{13,5},{2,10},{6,14},... | collective-permute-start | bytes 1572872 | tf_op jit(solution)/shard_map/ppermute | solution.py:417
  68.6 2.6 %collective-permute-start.5 = (bf16[1024,256]{1,0:T(8,128)(2,1)}, bf16[1024,256]{1,0:T(8,128)(2,1)S(1)}, u32[]{:S(2)}, u32[]{:S(2)}) collective-permute-start(bf16[1024,256]{1,0:T(8,128)(2,1)} %copy-done.22), channel_id=1, source_target_pairs={{0,4},{4,8},{8,12},{12,0},{1,5},{5,9},{9,13},{13,1},{2,6},{6,10},{... | collective-permute-start | bytes 1572872 | tf_op jit(solution)/shard_map/ppermute | solution.py:417
  71.2 17.8 %collective-permute-done.3.w1.w1_ref = bf16[1024,256]{1,0:T(8,128)(2,1)S(1)} collective-permute-done((bf16[1024,256]{1,0:T(8,128)(2,1)}, bf16[1024,256]{1,0:T(8,128)(2,1)S(1)}, u32[]{:S(2)}, u32[]{:S(2)}) %collective-permute-start.3) | collective-permute-done | bytes 524320 | tf_op jit(solution)/shard_map/ppermute | solution.py:417
  89.1 0.8 copy-done
  89.8 5.2 %collective-permute-done.5.w3.w3_ref = bf16[1024,256]{1,0:T(8,128)(2,1)S(1)} collective-permute-done((bf16[1024,256]{1,0:T(8,128)(2,1)}, bf16[1024,256]{1,0:T(8,128)(2,1)S(1)}, u32[]{:S(2)}, u32[]{:S(2)}) %collective-permute-start.5) | collective-permute-done | bytes 524320 | tf_op jit(solution)/shard_map/ppermute | solution.py:417
  95.1 0.8 copy-done.3
  95.9 1.0 copy-done.1
  96.9 1.0 copy-done.4
  98.0 1.5 gate_up.1
  99.5 14.3 %all_to_all.25.parts_ref = bf16[4,768,128]{2,1,0:T(8,128)(2,1)S(1)} all-to-all(bf16[4,768,128]{2,1,0:T(8,128)(2,1)S(1)} %gate_up.1), channel_id=1, replica_groups=mesh['z'=16,'core'=2,'y'=4,'x'=4] {'y'}, dimensions={0} | all-to-all | bytes 1572864 | tf_op jit(solution)/shard_map/all_to_all | solution.py:443
  113.8 1.6 hidden.1
  115.4 4.8 %all-to-all-start.3 = ((bf16[16,384,128]{2,1,0:T(8,128)(2,1)}), bf16[16,384,128]{2,1,0:T(8,128)(2,1)S(1)}, u32[]{:S(2)}, u32[]{:S(2)}) async-start(bf16[16,384,128]{2,1,0:T(8,128)(2,1)} %hidden.1), calls=%async_computation.3 | async-start | bytes 3145728 | tf_op jit(solution)/shard_map/all_to_all | solution.py:450
  120.3 0.9 copy-done.14
  121.2 2.2 %copy-done.21 = bf16[16384,128]{1,0:T(8,128)(2,1)S(1)} copy-done((bf16[16384,128]{1,0:T(8,128)(2,1)S(1)}, bf16[16384,128]{1,0:T(8,128)(2,1)}, u32[]{:S(2)}) %copy-start.21) | copy-done | bytes 4194328
  123.4 18.8 %attend.1.a0.after_ref = bf16[512,128]{1,0:T(8,128)(2,1)S(1)} custom-call(bf16[64,1024]{1,0:T(8,128)(2,1)S(1)} %copy-done.14, bf16[16384,128]{1,0:T(8,128)(2,1)S(1)} %copy-done.21), custom_call_target="tpu_custom_call" | custom-call | flops 4294967296 | bytes 4194304 | tf_op jit(solution)/shard_map/attend/pallas_call | solution.py:453
  142.2 1.0 copy-done.12
  143.2 1.0 down.1
  144.2 0.7 copy-done.6
  144.9 8.8 %all-to-all-start.4 = ((bf16[32,24,256]{2,1,0:T(8,128)(2,1)}), bf16[32,24,256]{2,1,0:T(8,128)(2,1)S(1)}, u32[]{:S(2)}, u32[]{:S(2)}) async-start(bf16[32,24,256]{2,1,0:T(8,128)(2,1)} %bitcast.20), calls=%async_computation.4 | async-start | bytes 786432 | tf_op jit(solution)/shard_map/all_to_all | solution.py:491
  153.8 3.4 %collective-permute-start.2 = (bf16[512,128]{1,0:T(8,128)(2,1)S(1)}, bf16[512,128]{1,0:T(8,128)(2,1)S(1)}, u32[]{:S(2)}, u32[]{:S(2)}) collective-permute-start(bf16[512,128]{1,0:T(8,128)(2,1)S(1)} %attend.1.a0.after_ref), channel_id=1, source_target_pairs={{0,3},{1,2},{2,1},{3,0},{4,7},{5,6},{6,5},{7,4},{8,11},{9,10},{10,... | collective-permute-start | bytes 393224 | tf_op jit(solution)/shard_map/ppermute | solution.py:478
  157.2 2.5 %collective-permute-start.1 = (bf16[512,128]{1,0:T(8,128)(2,1)S(1)}, bf16[512,128]{1,0:T(8,128)(2,1)S(1)}, u32[]{:S(2)}, u32[]{:S(2)}) collective-permute-start(bf16[512,128]{1,0:T(8,128)(2,1)S(1)} %attend.1.a0.after_ref), channel_id=1, source_target_pairs={{0,2},{1,3},{2,0},{3,1},{4,6},{5,7},{6,4},{7,5},{8,10},{9,11},{10,... | collective-permute-start | bytes 393224 | tf_op jit(solution)/shard_map/ppermute | solution.py:478
  159.7 3.1 %collective-permute-start = (bf16[512,128]{1,0:T(8,128)(2,1)S(1)}, bf16[512,128]{1,0:T(8,128)(2,1)S(1)}, u32[]{:S(2)}, u32[]{:S(2)}) collective-permute-start(bf16[512,128]{1,0:T(8,128)(2,1)S(1)} %attend.1.a0.after_ref), channel_id=1, source_target_pairs={{0,1},{1,0},{2,3},{3,2},{4,5},{5,4},{6,7},{7,6},{8,9},{9,8},{10,11... | collective-permute-start | bytes 393224 | tf_op jit(solution)/shard_map/ppermute | solution.py:478
  162.8 1.0 copy-done.2
  163.8 1.0 copy-done.5
  164.9 0.6 weights.1.w_ref
  165.5 1.5 collective-permute-done.a1
  167.1 0.7 mixer.1
  167.8 1.9 collective-permute-start.6
  169.7 4.2 %collective-permute-start.7 = (bf16[512,256]{1,0:T(8,128)(2,1)S(1)}, bf16[512,256]{1,0:T(8,128)(2,1)S(1)}, u32[]{:S(2)}, u32[]{:S(2)}) collective-permute-start(bf16[512,256]{1,0:T(8,128)(2,1)S(1)} %get-tuple-element.21), channel_id=1, source_target_pairs={{0,8},{4,12},{8,0},{12,4},{1,9},{5,13},{9,1},{13,5},{2,10},{6,14},... | collective-permute-start | bytes 786440 | tf_op jit(solution)/shard_map/ppermute | solution.py:512
  173.9 3.1 %collective-permute-start.8 = (bf16[512,256]{1,0:T(8,128)(2,1)S(1)}, bf16[512,256]{1,0:T(8,128)(2,1)S(1)}, u32[]{:S(2)}, u32[]{:S(2)}) collective-permute-start(bf16[512,256]{1,0:T(8,128)(2,1)S(1)} %get-tuple-element.22), channel_id=1, source_target_pairs={{0,12},{4,0},{8,4},{12,8},{1,13},{5,1},{9,5},{13,9},{2,14},{6,2},{... | collective-permute-start | bytes 786440 | tf_op jit(solution)/shard_map/ppermute | solution.py:512
  177.0 1.7 collective-permute-done.6.r1_ref
  178.7 3.7 %collective-permute-done.7.r2_ref = bf16[512,256]{1,0:T(8,128)(2,1)S(1)} collective-permute-done((bf16[512,256]{1,0:T(8,128)(2,1)S(1)}, bf16[512,256]{1,0:T(8,128)(2,1)S(1)}, u32[]{:S(2)}, u32[]{:S(2)}) %collective-permute-start.7) | collective-permute-done | bytes 262176 | tf_op jit(solution)/shard_map/ppermute | solution.py:512
  182.4 3.3 %collective-permute-done.8.r3_ref = bf16[512,256]{1,0:T(8,128)(2,1)S(1)} collective-permute-done((bf16[512,256]{1,0:T(8,128)(2,1)S(1)}, bf16[512,256]{1,0:T(8,128)(2,1)S(1)}, u32[]{:S(2)}, u32[]{:S(2)}) %collective-permute-start.8) | collective-permute-done | bytes 262176 | tf_op jit(solution)/shard_map/ppermute | solution.py:512
  185.7 0.8 mixed.1
  186.5 1.0 combine.1
  (52 shorter events, 0.7 us)
Async XLA Ops:
  7.2 113.1 %all-gather.2.cloned.1.call-start = ((), (), s32[]{:S(2)}) async-start(), calls=%async_computation.5 | async-start | bytes 4325376 | tf_op jit(solution)/shard_map/all_gather | solution.py:394
  8.2 19.7 %copy-start.18 = (s32[256,2]{0,1:T(2,128)S(1)}, s32[256,2]{0,1:T(2,128)}, u32[]{:S(2)}) copy-start(s32[256,2]{0,1:T(2,128)} %param.21) | copy-start | bytes 6148
  8.2 19.7 %copy-start.19 = (f32[256,2]{0,1:T(2,128)S(1)}, f32[256,2]{0,1:T(2,128)}, u32[]{:S(2)}) copy-start(f32[256,2]{0,1:T(2,128)} %param.22) | copy-start | bytes 6148
  8.2 21.5 %copy-start.7 = (bf16[2048,256]{1,0:T(8,128)(2,1)S(1)}, bf16[2048,256]{1,0:T(8,128)(2,1)}, u32[]{:S(2)}) copy-start(bf16[2048,256]{1,0:T(8,128)(2,1)} %mixer_ref.1) | copy-start | bytes 3145732
  8.2 21.5 %copy-start.10 = (bf16[1,4096,64]{1,2,0:T(8,128)(2,1)S(1)}, bf16[1,4096,64]{1,2,0:T(8,128)(2,1)}, u32[]{:S(2)}) copy-start(bf16[1,4096,64]{1,2,0:T(8,128)(2,1)} %param.23) | copy-start | bytes 1572868
  11.9 20.7 %copy-start.8 = (f32[32,512]{1,0:T(8,128)S(1)}, f32[32,512]{1,0:T(8,128)}, u32[]{:S(2)}) copy-start(f32[32,512]{1,0:T(8,128)} %get-tuple-element.26.sin_ref.refs_5_) | copy-start | bytes 196612
  11.9 20.7 %copy-start.9 = (f32[32,512]{1,0:T(8,128)S(1)}, f32[32,512]{1,0:T(8,128)}, u32[]{:S(2)}) copy-start(f32[32,512]{1,0:T(8,128)} %get-tuple-element.27.cos_ref.refs_4_) | copy-start | bytes 196612
  11.9 20.7 %copy-start.17 = (bf16[512,128]{1,0:T(8,128)(2,1)S(1)}, bf16[512,128]{1,0:T(8,128)(2,1)}, u32[]{:S(2)}) copy-start(bf16[512,128]{1,0:T(8,128)(2,1)} %q_ref.1) | copy-start | bytes 393220
  12.0 20.7 %copy-start.20 = (f32[64]{0:T(128)S(1)}, f32[64]{0:T(128)}, u32[]{:S(2)}) copy-start(f32[64]{0:T(128)} %param.16) | copy-start | bytes 772
  12.0 34.8 %all-to-all-start = ((bf16[16,48,256]{2,1,0:T(8,128)(2,1)}), bf16[16,48,256]{2,1,0:T(8,128)(2,1)S(1)}, u32[]{:S(2)}, u32[]{:S(2)}) async-start(bf16[16,48,256]{2,1,0:T(8,128)(2,1)} %bitcast.29), calls=%async_computation | async-start | bytes 786432 | tf_op jit(solution)/shard_map/all_to_all | solution.py:397
  28.9 0.7 copy-start.15
  29.7 1.0 copy-start.11
  31.5 0.8 copy-start.22
  31.5 1.0 copy-start.23
  31.5 1.1 copy-start.24
  32.8 15.2 %copy-start.13 = (bf16[64,1024]{1,0:T(8,128)(2,1)}, bf16[64,1024]{1,0:T(8,128)(2,1)S(1)}, u32[]{:S(2)}) copy-start(bf16[64,1024]{1,0:T(8,128)(2,1)S(1)} %queries.1.refs_0_) | copy-start | bytes 393220
  48.1 47.8 %all-to-all-start.1 = ((bf16[8,384,256]{2,1,0:T(8,128)(2,1)}), bf16[8,384,256]{2,1,0:T(8,128)(2,1)S(1)}, u32[]{:S(2)}, u32[]{:S(2)}) async-start(bf16[8,384,256]{2,1,0:T(8,128)(2,1)} %spread.1), calls=%async_computation.1 | async-start | bytes 3145728 | tf_op jit(solution)/shard_map/all_to_all | solution.py:435
  61.6 27.4 %collective-permute-start.3 = (bf16[1024,256]{1,0:T(8,128)(2,1)}, bf16[1024,256]{1,0:T(8,128)(2,1)S(1)}, u32[]{:S(2)}, u32[]{:S(2)}) collective-permute-start(bf16[1024,256]{1,0:T(8,128)(2,1)} %copy-done.24), channel_id=1, source_target_pairs={{0,12},{4,0},{8,4},{12,8},{1,13},{5,1},{9,5},{13,9},{2,14},{6,2},{... | collective-permute-start | bytes 1572872 | tf_op jit(solution)/shard_map/ppermute | solution.py:417
  66.4 22.7 %collective-permute-start.4 = (bf16[1024,256]{1,0:T(8,128)(2,1)}, bf16[1024,256]{1,0:T(8,128)(2,1)S(1)}, u32[]{:S(2)}, u32[]{:S(2)}) collective-permute-start(bf16[1024,256]{1,0:T(8,128)(2,1)} %copy-done.23), channel_id=1, source_target_pairs={{0,8},{4,12},{8,0},{12,4},{1,9},{5,13},{9,1},{13,5},{2,10},{6,14},... | collective-permute-start | bytes 1572872 | tf_op jit(solution)/shard_map/ppermute | solution.py:417
  68.6 26.5 %collective-permute-start.5 = (bf16[1024,256]{1,0:T(8,128)(2,1)}, bf16[1024,256]{1,0:T(8,128)(2,1)S(1)}, u32[]{:S(2)}, u32[]{:S(2)}) collective-permute-start(bf16[1024,256]{1,0:T(8,128)(2,1)} %copy-done.22), channel_id=1, source_target_pairs={{0,4},{4,8},{8,12},{12,0},{1,5},{5,9},{9,13},{13,1},{2,6},{6,10},{... | collective-permute-start | bytes 1572872 | tf_op jit(solution)/shard_map/ppermute | solution.py:417
  89.0 0.8 copy-start
  95.1 0.8 copy-start.3
  95.9 1.0 copy-start.1
  96.9 1.0 copy-start.4
  115.4 26.7 %all-to-all-start.3 = ((bf16[16,384,128]{2,1,0:T(8,128)(2,1)}), bf16[16,384,128]{2,1,0:T(8,128)(2,1)S(1)}, u32[]{:S(2)}, u32[]{:S(2)}) async-start(bf16[16,384,128]{2,1,0:T(8,128)(2,1)} %hidden.1), calls=%async_computation.3 | async-start | bytes 3145728 | tf_op jit(solution)/shard_map/all_to_all | solution.py:450
  120.3 0.9 copy-start.14
  121.2 2.2 %copy-start.21 = (bf16[16384,128]{1,0:T(8,128)(2,1)S(1)}, bf16[16384,128]{1,0:T(8,128)(2,1)}, u32[]{:S(2)}) copy-start(bf16[16384,128]{1,0:T(8,128)(2,1)} %all-gather.2.cloned.1.call-done.refs_1_) | copy-start | bytes 12582916
  142.1 1.0 copy-start.12
  144.2 0.7 copy-start.6
  144.9 41.6 %all-to-all-start.4 = ((bf16[32,24,256]{2,1,0:T(8,128)(2,1)}), bf16[32,24,256]{2,1,0:T(8,128)(2,1)S(1)}, u32[]{:S(2)}, u32[]{:S(2)}) async-start(bf16[32,24,256]{2,1,0:T(8,128)(2,1)} %bitcast.20), calls=%async_computation.4 | async-start | bytes 786432 | tf_op jit(solution)/shard_map/all_to_all | solution.py:491
  153.8 11.7 %collective-permute-start.2 = (bf16[512,128]{1,0:T(8,128)(2,1)S(1)}, bf16[512,128]{1,0:T(8,128)(2,1)S(1)}, u32[]{:S(2)}, u32[]{:S(2)}) collective-permute-start(bf16[512,128]{1,0:T(8,128)(2,1)S(1)} %attend.1.a0.after_ref), channel_id=1, source_target_pairs={{0,3},{1,2},{2,1},{3,0},{4,7},{5,6},{6,5},{7,4},{8,11},{9,10},{10,... | collective-permute-start | bytes 393224 | tf_op jit(solution)/shard_map/ppermute | solution.py:478
  157.2 8.4 %collective-permute-start.1 = (bf16[512,128]{1,0:T(8,128)(2,1)S(1)}, bf16[512,128]{1,0:T(8,128)(2,1)S(1)}, u32[]{:S(2)}, u32[]{:S(2)}) collective-permute-start(bf16[512,128]{1,0:T(8,128)(2,1)S(1)} %attend.1.a0.after_ref), channel_id=1, source_target_pairs={{0,2},{1,3},{2,0},{3,1},{4,6},{5,7},{6,4},{7,5},{8,10},{9,11},{10,... | collective-permute-start | bytes 393224 | tf_op jit(solution)/shard_map/ppermute | solution.py:478
  159.7 7.4 %collective-permute-start = (bf16[512,128]{1,0:T(8,128)(2,1)S(1)}, bf16[512,128]{1,0:T(8,128)(2,1)S(1)}, u32[]{:S(2)}, u32[]{:S(2)}) collective-permute-start(bf16[512,128]{1,0:T(8,128)(2,1)S(1)} %attend.1.a0.after_ref), channel_id=1, source_target_pairs={{0,1},{1,0},{2,3},{3,2},{4,5},{5,4},{6,7},{7,6},{8,9},{9,8},{10,11... | collective-permute-start | bytes 393224 | tf_op jit(solution)/shard_map/ppermute | solution.py:478
  162.8 1.0 copy-start.2
  163.8 1.0 copy-start.5
  165.5 21.0 %copy-start.16 = (f32[2,256,128]{2,1,0:T(8,128)S(1)}, f32[2,256,128]{2,1,0:T(8,128)}, u32[]{:S(2)}) copy-start(f32[2,256,128]{2,1,0:T(8,128)} %copy-done.15) | copy-start | bytes 786436
  167.8 10.9 %collective-permute-start.6 = (bf16[512,256]{1,0:T(8,128)(2,1)S(1)}, bf16[512,256]{1,0:T(8,128)(2,1)S(1)}, u32[]{:S(2)}, u32[]{:S(2)}) collective-permute-start(bf16[512,256]{1,0:T(8,128)(2,1)S(1)} %get-tuple-element.20), channel_id=1, source_target_pairs={{0,4},{4,8},{8,12},{12,0},{1,5},{5,9},{9,13},{13,1},{2,6},{6,10},{... | collective-permute-start | bytes 786440 | tf_op jit(solution)/shard_map/ppermute | solution.py:512
  169.7 12.7 %collective-permute-start.7 = (bf16[512,256]{1,0:T(8,128)(2,1)S(1)}, bf16[512,256]{1,0:T(8,128)(2,1)S(1)}, u32[]{:S(2)}, u32[]{:S(2)}) collective-permute-start(bf16[512,256]{1,0:T(8,128)(2,1)S(1)} %get-tuple-element.21), channel_id=1, source_target_pairs={{0,8},{4,12},{8,0},{12,4},{1,9},{5,13},{9,1},{13,5},{2,10},{6,14},... | collective-permute-start | bytes 786440 | tf_op jit(solution)/shard_map/ppermute | solution.py:512
  173.9 11.7 %collective-permute-start.8 = (bf16[512,256]{1,0:T(8,128)(2,1)S(1)}, bf16[512,256]{1,0:T(8,128)(2,1)S(1)}, u32[]{:S(2)}, u32[]{:S(2)}) collective-permute-start(bf16[512,256]{1,0:T(8,128)(2,1)S(1)} %get-tuple-element.22), channel_id=1, source_target_pairs={{0,12},{4,0},{8,4},{12,8},{1,13},{5,1},{9,5},{13,9},{2,14},{6,2},{... | collective-permute-start | bytes 786440 | tf_op jit(solution)/shard_map/ppermute | solution.py:512
Sparse Core Ops, SparseCore 0:
  12.1 86.0 all-gather.1

commit v4 on v3

--- a/solution.py
+++ b/solution.py
@@ -158,7 +158,8 @@
         out_ref[...] = acc.astype(out_ref.dtype)
 
 
-def mixed_body(own_ref, r1_ref, r2_ref, r3_ref, out_ref):
+def mixed_body(own_ref, r1_ref, r2_ref, r3_ref, after_ref, out_ref):
+    del after_ref
     total = own_ref[...]
     for ref in (r1_ref, r2_ref, r3_ref):
         total = total + ref[...].astype(f32)
@@ -510,19 +511,20 @@
     sums = [mixed[0]]
     for d in range(1, ny):
         sums.append(lax.ppermute(mixed[d], "y", [(i, (i + d) % ny) for i in range(ny)]))
+    moe_out = pl.pallas_call(
+        combine_body,
+        out_shape=jax.ShapeDtypeStruct((tokens, width), bf16),
+        compiler_params=params(),
+        name="combine",
+    )(returned, pick, share)
     attn_mixed = pl.pallas_call(
         mixed_body,
         out_shape=jax.ShapeDtypeStruct((seq, features), bf16),
+        in_specs=[vmem] * 4 + [anywhere],
         compiler_params=params(),
         name="mixed",
-    )(*sums)
-
-    moe_out = pl.pallas_call(
-        combine_body,
-        out_shape=jax.ShapeDtypeStruct((tokens, width), bf16),
-        compiler_params=params(),
-        name="combine",
-    )(returned, pick, share)
+    )(*sums, moe_out[:8, :128])
+
     return (attn_mixed, moe_out)
 
 

time: 196 us -> 196 us (level)
    ppermute x3, waiting for transfers between devices: 8.64 us -> 2.97 us  [on_device(): lax.ppermute(mixed[d], 'y', [(i, (i + d) % ny) for i in range(ny)])]
    all_to_all x1, waiting for transfers between devices: 0.01 us -> 3.95 us  [on_device(): lax.all_to_all(expert_out.reshape(ep, cap, width), EP, split_axis=0, conc...]
  transfers between devices with their start and end apart: 14 -> 14, of which waited for: 7 -> 6; matrix products, arithmetic and copies ran while one was open for 0% -> 0% of each run, Pallas kernels for 14% -> 14%
where the time goes in v4:
time: 196 us; the launch traced here: 194 us
  starting transfers between devices  70.9 us (36%)
  waiting for transfers between devices  45.5 us (23%)
  Pallas kernels  33.5 us (17%)
  between operations  14.4 us (7%)
  blocking collectives  14.3 us (7%)
  local copies, waits for them, and re-layouts  14.2 us (7%)
    ppermute x3, waiting for transfers between devices, on_device(): lax.ppermute(packs[d], 'y', [(i, (i - d) % ny) for i in range(ny)])  23.1 us
    pallas_call x1, Pallas kernels, on_device(): pl.pallas_call(lambda *refs: attend_body(*refs, n=seq, hw=hw, tile=256),...  18.8 us
    all_to_all x1, starting transfers between devices, on_device(): lax.all_to_all(own.reshape(nz, 2 * cap, width), 'z', split_axis=0, concat...  15.9 us
    all_to_all x1, blocking collectives, on_device(): lax.all_to_all(partial, 'y', split_axis=0, concat_axis=0, tiled=True)  14.3 us
    all_to_all x1, waiting for transfers between devices, on_device(): lax.all_to_all(own.reshape(nz, 2 * cap, width), 'z', split_axis=0, concat...  13.9 us
    unnamed x50, local copies, waits for them, and re-layouts  13.6 us
    all_to_all x1, starting transfers between devices, on_device(): lax.all_to_all(block, ('core', 'x'), split_axis=0, concat_axis=0, tiled=T...  13.6 us
    ppermute x3, starting transfers between devices, on_device(): lax.ppermute(packs[d], 'y', [(i, (i - d) % ny) for i in range(ny)])  9.57 us
  transfers between devices with their start and end apart: 14, of which 6 were waited for; matrix products, arithmetic and copies ran while one was open for 0% of the time, Pallas kernels for 14%

profile of v4, /device:TPU:1, one launch (start us, length us, event | category | flops | bytes accessed | tf_op | source)
XLA Modules:
  0.0 193.9 jit_solution(17449743292810798161)
XLA Ops:
  7.3 0.9 fusion
  8.2 3.7 %front.1 = (bf16[512,128]{1,0:T(8,128)(2,1)}, bf16[768,256]{1,0:T(8,128)(2,1)}) custom-call(s32[1]{0:T(128)} %bitcast.1.refs_0_, bf16[64,512]{1,0:T(8,128)(2,1)} %bitcast.30, bf16[64,512]{1,0:T(8,128)(2,1)} %bitcast.31, f32[1,64]{1,0:T(1,128)} %bitcast.33, f32[32,512]{1,0:T(8,128)} %get-tuple-element.27.cos_ref.refs_4_, ...), custom_call_target="tpu_custom_call" | custom-call | tf_op jit(solution)/shard_map/front/pallas_call | solution.py:383
  12.0 15.9 %all-to-all-start = ((bf16[16,48,256]{2,1,0:T(8,128)(2,1)}), bf16[16,48,256]{2,1,0:T(8,128)(2,1)S(1)}, u32[]{:S(2)}, u32[]{:S(2)}) async-start(bf16[16,48,256]{2,1,0:T(8,128)(2,1)} %bitcast.29), calls=%async_computation | async-start | bytes 786432 | tf_op jit(solution)/shard_map/all_to_all | solution.py:398
  27.9 1.0 routing.1
  28.9 0.7 copy-done.15
  29.7 1.0 copy-done.11
  30.7 0.7 pack.1
  31.5 0.8 copy-done.22
  32.6 0.2 queries.1.refs_0_
  32.9 13.9 %all-to-all-done.x_ref = bf16[16,48,256]{2,1,0:T(8,128)(2,1)S(1)} async-done(((bf16[16,48,256]{2,1,0:T(8,128)(2,1)}), bf16[16,48,256]{2,1,0:T(8,128)(2,1)S(1)}, u32[]{:S(2)}, u32[]{:S(2)}) %all-to-all-start) | async-done | bytes 393248 | tf_op jit(solution)/shard_map/all_to_all | solution.py:398
  46.8 1.3 spread.1
  48.1 13.6 %all-to-all-start.1 = ((bf16[8,384,256]{2,1,0:T(8,128)(2,1)}), bf16[8,384,256]{2,1,0:T(8,128)(2,1)S(1)}, u32[]{:S(2)}, u32[]{:S(2)}) async-start(bf16[8,384,256]{2,1,0:T(8,128)(2,1)} %spread.1), calls=%async_computation.1 | async-start | bytes 3145728 | tf_op jit(solution)/shard_map/all_to_all | solution.py:436
  61.6 4.7 %collective-permute-start.3 = (bf16[1024,256]{1,0:T(8,128)(2,1)}, bf16[1024,256]{1,0:T(8,128)(2,1)S(1)}, u32[]{:S(2)}, u32[]{:S(2)}) collective-permute-start(bf16[1024,256]{1,0:T(8,128)(2,1)} %copy-done.24), channel_id=1, source_target_pairs={{0,12},{4,0},{8,4},{12,8},{1,13},{5,1},{9,5},{13,9},{2,14},{6,2},{... | collective-permute-start | bytes 1572872 | tf_op jit(solution)/shard_map/ppermute | solution.py:418
  66.4 2.2 %collective-permute-start.4 = (bf16[1024,256]{1,0:T(8,128)(2,1)}, bf16[1024,256]{1,0:T(8,128)(2,1)S(1)}, u32[]{:S(2)}, u32[]{:S(2)}) collective-permute-start(bf16[1024,256]{1,0:T(8,128)(2,1)} %copy-done.23), channel_id=1, source_target_pairs={{0,8},{4,12},{8,0},{12,4},{1,9},{5,13},{9,1},{13,5},{2,10},{6,14},... | collective-permute-start | bytes 1572872 | tf_op jit(solution)/shard_map/ppermute | solution.py:418
  68.6 2.6 %collective-permute-start.5 = (bf16[1024,256]{1,0:T(8,128)(2,1)}, bf16[1024,256]{1,0:T(8,128)(2,1)S(1)}, u32[]{:S(2)}, u32[]{:S(2)}) collective-permute-start(bf16[1024,256]{1,0:T(8,128)(2,1)} %copy-done.22), channel_id=1, source_target_pairs={{0,4},{4,8},{8,12},{12,0},{1,5},{5,9},{9,13},{13,1},{2,6},{6,10},{... | collective-permute-start | bytes 1572872 | tf_op jit(solution)/shard_map/ppermute | solution.py:418
  71.2 17.8 %collective-permute-done.3.w1.w1_ref = bf16[1024,256]{1,0:T(8,128)(2,1)S(1)} collective-permute-done((bf16[1024,256]{1,0:T(8,128)(2,1)}, bf16[1024,256]{1,0:T(8,128)(2,1)S(1)}, u32[]{:S(2)}, u32[]{:S(2)}) %collective-permute-start.3) | collective-permute-done | bytes 524320 | tf_op jit(solution)/shard_map/ppermute | solution.py:418
  89.1 0.8 copy-done
  89.8 5.2 %collective-permute-done.5.w3.w3_ref = bf16[1024,256]{1,0:T(8,128)(2,1)S(1)} collective-permute-done((bf16[1024,256]{1,0:T(8,128)(2,1)}, bf16[1024,256]{1,0:T(8,128)(2,1)S(1)}, u32[]{:S(2)}, u32[]{:S(2)}) %collective-permute-start.5) | collective-permute-done | bytes 524320 | tf_op jit(solution)/shard_map/ppermute | solution.py:418
  95.1 0.8 copy-done.3
  95.9 1.0 copy-done.1
  96.9 1.0 copy-done.4
  98.0 1.5 gate_up.1
  99.5 14.3 %all_to_all.25.parts_ref = bf16[4,768,128]{2,1,0:T(8,128)(2,1)S(1)} all-to-all(bf16[4,768,128]{2,1,0:T(8,128)(2,1)S(1)} %gate_up.1), channel_id=1, replica_groups=mesh['z'=16,'core'=2,'y'=4,'x'=4] {'y'}, dimensions={0} | all-to-all | bytes 1572864 | tf_op jit(solution)/shard_map/all_to_all | solution.py:444
  113.8 1.6 hidden.1
  115.4 4.8 %all-to-all-start.3 = ((bf16[16,384,128]{2,1,0:T(8,128)(2,1)}), bf16[16,384,128]{2,1,0:T(8,128)(2,1)S(1)}, u32[]{:S(2)}, u32[]{:S(2)}) async-start(bf16[16,384,128]{2,1,0:T(8,128)(2,1)} %hidden.1), calls=%async_computation.3 | async-start | bytes 3145728 | tf_op jit(solution)/shard_map/all_to_all | solution.py:451
  120.3 0.9 copy-done.14
  121.2 2.2 %copy-done.21 = bf16[16384,128]{1,0:T(8,128)(2,1)S(1)} copy-done((bf16[16384,128]{1,0:T(8,128)(2,1)S(1)}, bf16[16384,128]{1,0:T(8,128)(2,1)}, u32[]{:S(2)}) %copy-start.21) | copy-done | bytes 4194328
  123.4 18.8 %attend.1.a0.after_ref = bf16[512,128]{1,0:T(8,128)(2,1)S(1)} custom-call(bf16[64,1024]{1,0:T(8,128)(2,1)S(1)} %copy-done.14, bf16[16384,128]{1,0:T(8,128)(2,1)S(1)} %copy-done.21), custom_call_target="tpu_custom_call" | custom-call | flops 4294967296 | bytes 4194304 | tf_op jit(solution)/shard_map/attend/pallas_call | solution.py:454
  142.2 1.0 copy-done.12
  143.2 1.0 down.1
  144.2 0.7 copy-done.6
  144.9 8.8 %all-to-all-start.4 = ((bf16[32,24,256]{2,1,0:T(8,128)(2,1)}), bf16[32,24,256]{2,1,0:T(8,128)(2,1)S(1)}, u32[]{:S(2)}, u32[]{:S(2)}) async-start(bf16[32,24,256]{2,1,0:T(8,128)(2,1)} %bitcast.20), calls=%async_computation.4 | async-start | bytes 786432 | tf_op jit(solution)/shard_map/all_to_all | solution.py:492
  153.8 3.4 %collective-permute-start.2 = (bf16[512,128]{1,0:T(8,128)(2,1)S(1)}, bf16[512,128]{1,0:T(8,128)(2,1)S(1)}, u32[]{:S(2)}, u32[]{:S(2)}) collective-permute-start(bf16[512,128]{1,0:T(8,128)(2,1)S(1)} %attend.1.a0.after_ref), channel_id=1, source_target_pairs={{0,3},{1,2},{2,1},{3,0},{4,7},{5,6},{6,5},{7,4},{8,11},{9,10},{10,... | collective-permute-start | bytes 393224 | tf_op jit(solution)/shard_map/ppermute | solution.py:479
  157.2 2.5 %collective-permute-start.1 = (bf16[512,128]{1,0:T(8,128)(2,1)S(1)}, bf16[512,128]{1,0:T(8,128)(2,1)S(1)}, u32[]{:S(2)}, u32[]{:S(2)}) collective-permute-start(bf16[512,128]{1,0:T(8,128)(2,1)S(1)} %attend.1.a0.after_ref), channel_id=1, source_target_pairs={{0,2},{1,3},{2,0},{3,1},{4,6},{5,7},{6,4},{7,5},{8,10},{9,11},{10,... | collective-permute-start | bytes 393224 | tf_op jit(solution)/shard_map/ppermute | solution.py:479
  159.7 3.1 %collective-permute-start = (bf16[512,128]{1,0:T(8,128)(2,1)S(1)}, bf16[512,128]{1,0:T(8,128)(2,1)S(1)}, u32[]{:S(2)}, u32[]{:S(2)}) collective-permute-start(bf16[512,128]{1,0:T(8,128)(2,1)S(1)} %attend.1.a0.after_ref), channel_id=1, source_target_pairs={{0,1},{1,0},{2,3},{3,2},{4,5},{5,4},{6,7},{7,6},{8,9},{9,8},{10,11... | collective-permute-start | bytes 393224 | tf_op jit(solution)/shard_map/ppermute | solution.py:479
  162.8 1.0 copy-done.2
  163.8 1.0 copy-done.5
  164.9 0.6 weights.1.w_ref
  165.5 1.5 collective-permute-done.a1
  167.1 1.3 mixer.1
  168.3 1.9 collective-permute-start.6
  170.3 4.2 %collective-permute-start.7 = (bf16[512,256]{1,0:T(8,128)(2,1)S(1)}, bf16[512,256]{1,0:T(8,128)(2,1)S(1)}, u32[]{:S(2)}, u32[]{:S(2)}) collective-permute-start(bf16[512,256]{1,0:T(8,128)(2,1)S(1)} %get-tuple-element.21), channel_id=1, source_target_pairs={{0,8},{4,12},{8,0},{12,4},{1,9},{5,13},{9,1},{13,5},{2,10},{6,14},... | collective-permute-start | bytes 786440 | tf_op jit(solution)/shard_map/ppermute | solution.py:513
  174.5 3.1 %collective-permute-start.8 = (bf16[512,256]{1,0:T(8,128)(2,1)S(1)}, bf16[512,256]{1,0:T(8,128)(2,1)S(1)}, u32[]{:S(2)}, u32[]{:S(2)}) collective-permute-start(bf16[512,256]{1,0:T(8,128)(2,1)S(1)} %get-tuple-element.22), channel_id=1, source_target_pairs={{0,12},{4,0},{8,4},{12,8},{1,13},{5,1},{9,5},{13,9},{2,14},{6,2},{... | collective-permute-start | bytes 786440 | tf_op jit(solution)/shard_map/ppermute | solution.py:513
  177.6 3.9 %all-to-all-done.4 = bf16[32,24,256]{2,1,0:T(8,128)(2,1)S(1)} async-done(((bf16[32,24,256]{2,1,0:T(8,128)(2,1)}), bf16[32,24,256]{2,1,0:T(8,128)(2,1)S(1)}, u32[]{:S(2)}, u32[]{:S(2)}) %all-to-all-start.4) | async-done | bytes 393248 | tf_op jit(solution)/shard_map/all_to_all | solution.py:492
  181.5 1.0 combine.1
  182.6 0.7 slice.13.after_ref
  183.3 3.0 %collective-permute-done.8.r3_ref = bf16[512,256]{1,0:T(8,128)(2,1)S(1)} collective-permute-done((bf16[512,256]{1,0:T(8,128)(2,1)S(1)}, bf16[512,256]{1,0:T(8,128)(2,1)S(1)}, u32[]{:S(2)}, u32[]{:S(2)}) %collective-permute-start.8) | collective-permute-done | bytes 262176 | tf_op jit(solution)/shard_map/ppermute | solution.py:513
  186.2 0.8 mixed.1
  (53 shorter events, 0.7 us)
Async XLA Ops:
  7.2 113.1 %all-gather.2.cloned.1.call-start = ((), (), s32[]{:S(2)}) async-start(), calls=%async_computation.5 | async-start | bytes 4325376 | tf_op jit(solution)/shard_map/all_gather | solution.py:395
  8.2 19.7 %copy-start.18 = (s32[256,2]{0,1:T(2,128)S(1)}, s32[256,2]{0,1:T(2,128)}, u32[]{:S(2)}) copy-start(s32[256,2]{0,1:T(2,128)} %param.21) | copy-start | bytes 6148
  8.2 19.7 %copy-start.19 = (f32[256,2]{0,1:T(2,128)S(1)}, f32[256,2]{0,1:T(2,128)}, u32[]{:S(2)}) copy-start(f32[256,2]{0,1:T(2,128)} %param.22) | copy-start | bytes 6148
  8.2 21.5 %copy-start.7 = (bf16[2048,256]{1,0:T(8,128)(2,1)S(1)}, bf16[2048,256]{1,0:T(8,128)(2,1)}, u32[]{:S(2)}) copy-start(bf16[2048,256]{1,0:T(8,128)(2,1)} %mixer_ref.1) | copy-start | bytes 3145732
  8.2 21.5 %copy-start.10 = (bf16[1,4096,64]{1,2,0:T(8,128)(2,1)S(1)}, bf16[1,4096,64]{1,2,0:T(8,128)(2,1)}, u32[]{:S(2)}) copy-start(bf16[1,4096,64]{1,2,0:T(8,128)(2,1)} %param.23) | copy-start | bytes 1572868
  11.9 20.7 %copy-start.8 = (f32[32,512]{1,0:T(8,128)S(1)}, f32[32,512]{1,0:T(8,128)}, u32[]{:S(2)}) copy-start(f32[32,512]{1,0:T(8,128)} %get-tuple-element.26.sin_ref.refs_5_) | copy-start | bytes 196612
  11.9 20.7 %copy-start.9 = (f32[32,512]{1,0:T(8,128)S(1)}, f32[32,512]{1,0:T(8,128)}, u32[]{:S(2)}) copy-start(f32[32,512]{1,0:T(8,128)} %get-tuple-element.27.cos_ref.refs_4_) | copy-start | bytes 196612
  11.9 20.7 %copy-start.17 = (bf16[512,128]{1,0:T(8,128)(2,1)S(1)}, bf16[512,128]{1,0:T(8,128)(2,1)}, u32[]{:S(2)}) copy-start(bf16[512,128]{1,0:T(8,128)(2,1)} %q_ref.1) | copy-start | bytes 393220
  12.0 20.7 %copy-start.20 = (f32[64]{0:T(128)S(1)}, f32[64]{0:T(128)}, u32[]{:S(2)}) copy-start(f32[64]{0:T(128)} %param.16) | copy-start | bytes 772
  12.0 34.8 %all-to-all-start = ((bf16[16,48,256]{2,1,0:T(8,128)(2,1)}), bf16[16,48,256]{2,1,0:T(8,128)(2,1)S(1)}, u32[]{:S(2)}, u32[]{:S(2)}) async-start(bf16[16,48,256]{2,1,0:T(8,128)(2,1)} %bitcast.29), calls=%async_computation | async-start | bytes 786432 | tf_op jit(solution)/shard_map/all_to_all | solution.py:398
  28.9 0.7 copy-start.15
  29.7 1.0 copy-start.11
  31.5 0.8 copy-start.22
  31.5 1.0 copy-start.23
  31.5 1.1 copy-start.24
  32.8 15.2 %copy-start.13 = (bf16[64,1024]{1,0:T(8,128)(2,1)}, bf16[64,1024]{1,0:T(8,128)(2,1)S(1)}, u32[]{:S(2)}) copy-start(bf16[64,1024]{1,0:T(8,128)(2,1)S(1)} %queries.1.refs_0_) | copy-start | bytes 393220
  48.1 47.8 %all-to-all-start.1 = ((bf16[8,384,256]{2,1,0:T(8,128)(2,1)}), bf16[8,384,256]{2,1,0:T(8,128)(2,1)S(1)}, u32[]{:S(2)}, u32[]{:S(2)}) async-start(bf16[8,384,256]{2,1,0:T(8,128)(2,1)} %spread.1), calls=%async_computation.1 | async-start | bytes 3145728 | tf_op jit(solution)/shard_map/all_to_all | solution.py:436
  61.6 27.4 %collective-permute-start.3 = (bf16[1024,256]{1,0:T(8,128)(2,1)}, bf16[1024,256]{1,0:T(8,128)(2,1)S(1)}, u32[]{:S(2)}, u32[]{:S(2)}) collective-permute-start(bf16[1024,256]{1,0:T(8,128)(2,1)} %copy-done.24), channel_id=1, source_target_pairs={{0,12},{4,0},{8,4},{12,8},{1,13},{5,1},{9,5},{13,9},{2,14},{6,2},{... | collective-permute-start | bytes 1572872 | tf_op jit(solution)/shard_map/ppermute | solution.py:418
  66.4 22.7 %collective-permute-start.4 = (bf16[1024,256]{1,0:T(8,128)(2,1)}, bf16[1024,256]{1,0:T(8,128)(2,1)S(1)}, u32[]{:S(2)}, u32[]{:S(2)}) collective-permute-start(bf16[1024,256]{1,0:T(8,128)(2,1)} %copy-done.23), channel_id=1, source_target_pairs={{0,8},{4,12},{8,0},{12,4},{1,9},{5,13},{9,1},{13,5},{2,10},{6,14},... | collective-permute-start | bytes 1572872 | tf_op jit(solution)/shard_map/ppermute | solution.py:418
  68.6 26.5 %collective-permute-start.5 = (bf16[1024,256]{1,0:T(8,128)(2,1)}, bf16[1024,256]{1,0:T(8,128)(2,1)S(1)}, u32[]{:S(2)}, u32[]{:S(2)}) collective-permute-start(bf16[1024,256]{1,0:T(8,128)(2,1)} %copy-done.22), channel_id=1, source_target_pairs={{0,4},{4,8},{8,12},{12,0},{1,5},{5,9},{9,13},{13,1},{2,6},{6,10},{... | collective-permute-start | bytes 1572872 | tf_op jit(solution)/shard_map/ppermute | solution.py:418
  89.0 0.8 copy-start
  95.1 0.8 copy-start.3
  95.9 1.0 copy-start.1
  96.9 1.0 copy-start.4
  115.4 26.7 %all-to-all-start.3 = ((bf16[16,384,128]{2,1,0:T(8,128)(2,1)}), bf16[16,384,128]{2,1,0:T(8,128)(2,1)S(1)}, u32[]{:S(2)}, u32[]{:S(2)}) async-start(bf16[16,384,128]{2,1,0:T(8,128)(2,1)} %hidden.1), calls=%async_computation.3 | async-start | bytes 3145728 | tf_op jit(solution)/shard_map/all_to_all | solution.py:451
  120.3 0.9 copy-start.14
  121.2 2.2 %copy-start.21 = (bf16[16384,128]{1,0:T(8,128)(2,1)S(1)}, bf16[16384,128]{1,0:T(8,128)(2,1)}, u32[]{:S(2)}) copy-start(bf16[16384,128]{1,0:T(8,128)(2,1)} %all-gather.2.cloned.1.call-done.refs_1_) | copy-start | bytes 12582916
  142.1 1.0 copy-start.12
  144.2 0.7 copy-start.6
  144.9 36.6 %all-to-all-start.4 = ((bf16[32,24,256]{2,1,0:T(8,128)(2,1)}), bf16[32,24,256]{2,1,0:T(8,128)(2,1)S(1)}, u32[]{:S(2)}, u32[]{:S(2)}) async-start(bf16[32,24,256]{2,1,0:T(8,128)(2,1)} %bitcast.20), calls=%async_computation.4 | async-start | bytes 786432 | tf_op jit(solution)/shard_map/all_to_all | solution.py:492
  153.8 11.7 %collective-permute-start.2 = (bf16[512,128]{1,0:T(8,128)(2,1)S(1)}, bf16[512,128]{1,0:T(8,128)(2,1)S(1)}, u32[]{:S(2)}, u32[]{:S(2)}) collective-permute-start(bf16[512,128]{1,0:T(8,128)(2,1)S(1)} %attend.1.a0.after_ref), channel_id=1, source_target_pairs={{0,3},{1,2},{2,1},{3,0},{4,7},{5,6},{6,5},{7,4},{8,11},{9,10},{10,... | collective-permute-start | bytes 393224 | tf_op jit(solution)/shard_map/ppermute | solution.py:479
  157.2 8.4 %collective-permute-start.1 = (bf16[512,128]{1,0:T(8,128)(2,1)S(1)}, bf16[512,128]{1,0:T(8,128)(2,1)S(1)}, u32[]{:S(2)}, u32[]{:S(2)}) collective-permute-start(bf16[512,128]{1,0:T(8,128)(2,1)S(1)} %attend.1.a0.after_ref), channel_id=1, source_target_pairs={{0,2},{1,3},{2,0},{3,1},{4,6},{5,7},{6,4},{7,5},{8,10},{9,11},{10,... | collective-permute-start | bytes 393224 | tf_op jit(solution)/shard_map/ppermute | solution.py:479
  159.7 7.4 %collective-permute-start = (bf16[512,128]{1,0:T(8,128)(2,1)S(1)}, bf16[512,128]{1,0:T(8,128)(2,1)S(1)}, u32[]{:S(2)}, u32[]{:S(2)}) collective-permute-start(bf16[512,128]{1,0:T(8,128)(2,1)S(1)} %attend.1.a0.after_ref), channel_id=1, source_target_pairs={{0,1},{1,0},{2,3},{3,2},{4,5},{5,4},{6,7},{7,6},{8,9},{9,8},{10,11... | collective-permute-start | bytes 393224 | tf_op jit(solution)/shard_map/ppermute | solution.py:479
  162.8 1.0 copy-start.2
  163.8 1.0 copy-start.5
  165.5 16.0 %copy-start.16 = (f32[2,256,128]{2,1,0:T(8,128)S(1)}, f32[2,256,128]{2,1,0:T(8,128)}, u32[]{:S(2)}) copy-start(f32[2,256,128]{2,1,0:T(8,128)} %copy-done.15) | copy-start | bytes 786436
  168.3 14.9 %collective-permute-start.6 = (bf16[512,256]{1,0:T(8,128)(2,1)}, bf16[512,256]{1,0:T(8,128)(2,1)S(1)}, u32[]{:S(2)}, u32[]{:S(2)}) collective-permute-start(bf16[512,256]{1,0:T(8,128)(2,1)} %get-tuple-element.20), channel_id=1, source_target_pairs={{0,4},{4,8},{8,12},{12,0},{1,5},{5,9},{9,13},{13,1},{2,6},{6,10},{... | collective-permute-start | bytes 786440 | tf_op jit(solution)/shard_map/ppermute | solution.py:513
  170.3 13.0 %collective-permute-start.7 = (bf16[512,256]{1,0:T(8,128)(2,1)S(1)}, bf16[512,256]{1,0:T(8,128)(2,1)S(1)}, u32[]{:S(2)}, u32[]{:S(2)}) collective-permute-start(bf16[512,256]{1,0:T(8,128)(2,1)S(1)} %get-tuple-element.21), channel_id=1, source_target_pairs={{0,8},{4,12},{8,0},{12,4},{1,9},{5,13},{9,1},{13,5},{2,10},{6,14},... | collective-permute-start | bytes 786440 | tf_op jit(solution)/shard_map/ppermute | solution.py:513
  174.5 11.7 %collective-permute-start.8 = (bf16[512,256]{1,0:T(8,128)(2,1)S(1)}, bf16[512,256]{1,0:T(8,128)(2,1)S(1)}, u32[]{:S(2)}, u32[]{:S(2)}) collective-permute-start(bf16[512,256]{1,0:T(8,128)(2,1)S(1)} %get-tuple-element.22), channel_id=1, source_target_pairs={{0,12},{4,0},{8,4},{12,8},{1,13},{5,1},{9,5},{13,9},{2,14},{6,2},{... | collective-permute-start | bytes 786440 | tf_op jit(solution)/shard_map/ppermute | solution.py:513
Sparse Core Ops, SparseCore 0:
  12.1 86.0 all-gather.1
